TPU v7x, 128 devices: a whole 4x4x4 slice. The times are simulated.
128 devices in a mesh: fs: 16 (over z, x), tp: 8 (over y, core).
Axes of the slice: x: 4, y: 4, z: 4, core: 2. Of those that a mesh axis runs over, the one named last changes fastest.
Arguments:
- resid: bfloat16 [16384, 2048], P(('fs', 'tp')), may hold values from -6 to 6
- mix_gain: float32 [2048], replicated, may hold values from 0.1 to 1.9
- in_weight: bfloat16 [2048, 2048], P('fs', 'tp'), may hold values from -0.125 to 0.125
- conv_taps: float32 [4, 2048], P(None, 'tp'), may hold values from -3 to 3
- recur_gate_w: bfloat16 [32, 64, 64], P('tp'), may hold values from -0.75 to 0.75
- input_gate_w: bfloat16 [32, 64, 64], P('tp'), may hold values from -0.75 to 0.75
- decay_rate: float32 [2048], P('tp'), may hold values from 0.0004 to 0.03
- out_weight: bfloat16 [2048, 2048], P('tp', 'fs'), may hold values from -0.25 to 0.25
- mlp_gain: float32 [2048], replicated, may hold values from 0.1 to 1.9
- up_gate_w: bfloat16 [2048, 5632], P('fs', 'tp'), may hold values from -0.125 to 0.125
- up_val_w: bfloat16 [2048, 5632], P('fs', 'tp'), may hold values from -0.125 to 0.125
- ffn_taps: float32 [3, 5632], P(None, 'tp'), may hold values from -3 to 3
- down_weight: bfloat16 [5632, 2048], P('tp', 'fs'), may hold values from -0.15625 to 0.15625
Outputs:
- result: bfloat16 [16384, 2048], P(('fs', 'tp'))
All inputs are finite; a program needn't handle non-finite values.
Results may differ from a plain program's by a relative error of at most 0.028.
Values may be sent and summed in bfloat16 or wider, within the bound.
A program may use at most 64 MiB of HBM per device.

v0:
```python
import jax
import jax.numpy as jnp
from jax import lax
from jax.sharding import Mesh
from jax.sharding import PartitionSpec as P

GATE_BLOCK = 64
SEQ_LEN = 128
FS = ("fs_0", "fs_1")
FS_TP = ("fs_0", "fs_1", "tp")


def copy_for_each(shard, axis):
    size = lax.axis_size(axis)
    return lax.all_to_all(
        jnp.broadcast_to(shard[None], (size, *shard.shape)), axis, 0, 0, tiled=True
    )


def joined_along(pieces, dim):
    lengths = list(pieces.shape[1:])
    lengths[dim] *= pieces.shape[0]
    return jnp.moveaxis(pieces, 0, dim).reshape(lengths)


def gather_directly(shard, axis, dim):
    pieces = copy_for_each(shard, axis)
    return joined_along(pieces, dim)


def in_blocks(shard, dim, size):
    lengths = shard.shape
    pieces = shard.reshape(*lengths[:dim], size, lengths[dim] // size, *lengths[dim + 1 :])
    return jnp.moveaxis(pieces, dim, 0)


def sent_and_summed(shard, axis, dim):
    size = lax.axis_size(axis)
    pieces = lax.all_to_all(in_blocks(shard, dim, size), axis, 0, 0, tiled=True)
    return jnp.sum(pieces.astype(jnp.float32), axis=0)


def in_one_piece(arrays, axis, dim, along):
    ends, at = ([], 0)
    for a in arrays[:-1]:
        at += a.shape[along]
        ends.append(at)
    both = jnp.concatenate(arrays, axis=along)
    return tuple(jnp.split(lax.all_gather(both, axis, axis=dim, tiled=True), ends, axis=along))


def gathered_by_axis(shard, axes, dim):
    for axis in reversed(axes):
        shard = lax.all_gather(shard, axis, axis=dim, tiled=True)
    return shard


def rms_scale(rows_in, gain_vec):
    wide = rows_in.astype(jnp.float32)
    return wide * lax.rsqrt(jnp.mean(wide * wide, axis=-1, keepdims=True) + 1e-06) * gain_vec


def causal_taps(values, tap_weights):
    width = tap_weights.shape[0]
    length = values.shape[1]
    padded = jnp.pad(values, ((0, 0), (width - 1, 0), (0, 0)))
    summed = jnp.zeros_like(values)
    for tap_index in range(width):
        summed = summed + padded[:, tap_index : tap_index + length] * tap_weights[tap_index]
    return summed


def combine(earlier, later):
    return (earlier[0] * later[0], later[0] * earlier[1] + later[1])


def recurrence(projected, conv_taps, recur_gate_w, input_gate_w, decay_rate):
    channels = projected.shape[1]
    seqs = projected.shape[0] // SEQ_LEN
    nblock = recur_gate_w.shape[0]
    conv = causal_taps(projected.astype(jnp.float32).reshape(seqs, SEQ_LEN, channels), conv_taps)
    blocks = conv.astype(jnp.bfloat16).reshape(seqs, SEQ_LEN, nblock, GATE_BLOCK)
    rgate = jax.nn.sigmoid(
        jnp.einsum(
            "slnd,nde->slne", blocks, recur_gate_w, preferred_element_type=jnp.float32
        ).reshape(seqs, SEQ_LEN, channels)
    )
    igate = jax.nn.sigmoid(
        jnp.einsum(
            "slnd,nde->slne", blocks, input_gate_w, preferred_element_type=jnp.float32
        ).reshape(seqs, SEQ_LEN, channels)
    )
    logdecay = -8.0 * rgate * decay_rate
    decay = jnp.exp(logdecay)
    drive = jnp.sqrt(-jnp.expm1(2.0 * logdecay)) * (igate * conv)
    state = lax.associative_scan(combine, (decay, drive), axis=1)[1]
    return state.astype(jnp.bfloat16).reshape(seqs * SEQ_LEN, channels)


def shards(
    resid,
    mix_gain,
    in_weight,
    conv_taps,
    recur_gate_w,
    input_gate_w,
    decay_rate,
    out_weight,
    mlp_gain,
    up_gate_w,
    up_val_w,
    ffn_taps,
    down_weight,
):
    normed = rms_scale(resid, mix_gain).astype(jnp.bfloat16)
    gathered = lax.all_gather(normed, "tp", axis=0, tiled=True)
    columns = gathered
    projected = jnp.dot(
        columns, gather_directly(in_weight, FS, 0), preferred_element_type=jnp.float32
    ).astype(jnp.bfloat16)
    recurred = recurrence(projected, conv_taps, recur_gate_w, input_gate_w, decay_rate)
    partial_mix = jnp.dot(
        recurred, gather_directly(out_weight, FS, 1), preferred_element_type=jnp.float32
    )
    mixed_sum = sent_and_summed(partial_mix.astype(jnp.bfloat16), "tp", 0)
    middle = (resid.astype(jnp.float32) + mixed_sum).astype(jnp.bfloat16)
    normed_two = rms_scale(middle, mlp_gain).astype(jnp.bfloat16)
    local_hidden = up_gate_w.shape[1]
    gathered_two = lax.all_gather(normed_two, "tp", axis=0, tiled=True)
    portions = in_one_piece((up_gate_w, up_val_w), FS, 0, 1)
    columns = gathered_two
    gate_wide = jnp.dot(columns, portions[0], preferred_element_type=jnp.float32)
    value_wide = jnp.dot(columns, portions[1], preferred_element_type=jnp.float32)
    gate_pre = gate_wide.astype(jnp.bfloat16)
    value_pre = value_wide.astype(jnp.bfloat16)
    seqs = gate_pre.shape[0] // SEQ_LEN
    gate_conv = causal_taps(
        gate_pre.astype(jnp.float32).reshape(seqs, SEQ_LEN, local_hidden), ffn_taps
    ).reshape(seqs * SEQ_LEN, local_hidden)
    hidden = (jax.nn.silu(gate_conv) * value_pre.astype(jnp.float32)).astype(jnp.bfloat16)
    partial_down = jnp.dot(
        hidden, gathered_by_axis(down_weight, FS, 1), preferred_element_type=jnp.float32
    )
    ffn_sum = sent_and_summed(partial_down.astype(jnp.bfloat16), "tp", 0)
    return (middle.astype(jnp.float32) + ffn_sum).astype(jnp.bfloat16)


def solution(mesh):
    split = Mesh(mesh.devices.reshape(4, 4, mesh.shape["tp"]), ("fs_0", "fs_1", "tp"))
    return jax.shard_map(
        shards,
        mesh=split,
        in_specs=(
            P(FS_TP, None),
            P(),
            P(FS, "tp"),
            P(None, "tp"),
            P("tp", None, None),
            P("tp", None, None),
            P("tp"),
            P("tp", FS),
            P(),
            P(FS, "tp"),
            P(FS, "tp"),
            P(None, "tp"),
            P("tp", FS),
        ),
        out_specs=P(FS_TP, None),
        check_vma=False,
    )
```

profile of v0, /device:TPU:1, one launch (start us, length us, event | category | flops | bytes accessed | tf_op | source)
XLA Modules:
  0.0 283.8 jit_solution(2252259984730059512)
XLA Ops:
  6.5 1.3 fusion.33
  7.9 2.1 fusion.35
  10.0 1.9 broadcast_in_dim.4
  11.9 8.4 %all-to-all-start = ((bf16[16,128,256]{2,1,0:T(8,128)(2,1)}), bf16[16,128,256]{2,1,0:T(8,128)(2,1)S(1)}, u32[]{:S(2)}, u32[]{:S(2)}) async-start(bf16[16,128,256]{2,1,0:T(8,128)(2,1)} %broadcast_in_dim.4), calls=%async_computation | async-start | bytes 2097152 | tf_op jit(solution)/shard_map/all_to_all | solution.py:15
  20.4 0.7 pad_maximum_fusion.1
  21.1 0.1 copy.122
  21.3 15.0 %all-to-all-done = bf16[16,128,256]{2,1,0:T(8,128)(2,1)S(1)} async-done(((bf16[16,128,256]{2,1,0:T(8,128)(2,1)}), bf16[16,128,256]{2,1,0:T(8,128)(2,1)S(1)}, u32[]{:S(2)}, u32[]{:S(2)}) %all-to-all-start) | async-done | bytes 1048608 | tf_op jit(solution)/shard_map/all_to_all | solution.py:15
  36.3 1.1 broadcast_in_dim.5
  37.4 4.2 %all-to-all-start.1 = ((bf16[16,256,128]{1,2,0:T(8,128)(2,1)}), bf16[16,256,128]{1,2,0:T(8,128)(2,1)S(1)}, u32[]{:S(2)}, u32[]{:S(2)}) async-start(bf16[16,256,128]{1,2,0:T(8,128)(2,1)} %broadcast_in_dim.5), calls=%async_computation.1 | async-start | bytes 2097152 | tf_op jit(solution)/shard_map/all_to_all | solution.py:15
  41.6 4.1 %all-gather.5.cloned.1.call-done = bf16[1024,2048]{1,0:T(8,128)(2,1)} async-done(((bf16[128,2048]{1,0:T(8,128)(2,1)}), bf16[1024,2048]{1,0:T(8,128)(2,1)}) %all-gather.5.cloned.1.call-update) | async-done | bytes 4194320 | tf_op jit(solution)/shard_map/all_gather | solution.py:116
  45.8 3.4 %convolution_convert_fusion.2 = bf16[1024,256]{1,0:T(8,128)(2,1)S(1)} fusion(bf16[1024,2048]{1,0:T(8,128)(2,1)} %all-gather.5.cloned.1.call-done, bf16[2048,256]{1,0:T(8,128)(2,1)S(1)} %bitcast.80), kind=kOutput, calls=%fused_computation.40 | convolution fusion | flops 1074003968 | bytes 5767168 | tf_op jit(solution)/shard_map/dot_general | solution.py:118
  49.3 1.4 fusion.56
  50.8 0.3 copy.113
  51.0 0.5 fusion.30
  51.6 1.4 copy.121
  53.0 0.5 fusion.27
  53.6 1.3 copy.117
  54.9 2.6 multiply_exponential_fusion
  57.5 1.5 slice.210
  59.0 1.5 slice.206
  60.4 1.5 slice.205
  61.9 0.3 slice.254
  62.2 1.5 slice.208
  63.7 1.4 slice.207
  65.1 1.5 fusion.57
  66.6 0.1 slice.216
  66.8 0.1 slice.212
  66.9 0.2 slice.211
  67.1 0.2 slice.252
  67.3 0.1 slice.214
  67.4 0.8 slice.213
  68.2 1.0 fusion.58
  69.2 0.1 slice.222
  69.4 0.1 slice.218
  69.5 0.1 slice.217
  69.6 0.1 slice.250
  69.7 0.1 slice.220
  69.8 0.1 slice.219
  70.7 0.1 pad.54
  70.8 0.1 pad.55
  71.7 0.7 add.170
  72.5 0.2 pad.62
  72.7 3.1 %pad.63 = f32[8,64,256]{2,1,0:T(8,128)S(1)} pad(f32[8,32,256]{2,1,0:T(8,128)} %add.170, f32[]{:T(128)} %constant.7.clone.1), padding=0_0_0x1_0_1x0_0_0 | pad | bytes 786436 | tf_op jit(solution)/shard_map/pad | solution.py:96
  75.8 0.9 add.172
  76.7 0.1 fusion.42
  76.9 0.3 pad.64
  77.2 3.6 %pad.65 = f32[8,128,256]{2,1,0:T(8,128)S(1)} pad(f32[8,64,256]{2,1,0:T(8,128)} %add.172, f32[]{:T(128)} %constant.7.clone.1), padding=0_0_0x1_0_1x0_0_0 | pad | bytes 1572868 | tf_op jit(solution)/shard_map/pad | solution.py:96
  80.7 0.9 add_convert_fusion
  81.6 2.3 convolution_convert_fusion.1
  84.0 51.7 %all_to_all.20 = bf16[8,128,2048]{2,1,0:T(8,128)(2,1)S(1)} all-to-all(bf16[8,128,2048]{2,1,0:T(8,128)(2,1)S(1)} %bitcast.72), channel_id=1, replica_groups=mesh['fs_0'=4,'fs_1'=4,'tp'=8] {'tp'}, dimensions={0} | all-to-all | bytes 8388608 | tf_op jit(solution)/shard_map/all_to_all | solution.py:39
  135.7 0.7 convert_reduce_fusion.1
  136.4 0.3 copy-done.2
  136.7 0.2 fusion.37
  137.0 1.0 fusion.39
  138.1 15.1 %all_gather.18 = bf16[704,512]{1,0:T(8,128)(2,1)} all-gather(bf16[704,128]{1,0:T(8,128)(2,1)S(1)} %copy-done.5), channel_id=1, replica_groups=mesh['fs_0'=4,'fs_1'=4,'tp'=8] {'fs_1'}, dimensions={1}, use_global_device_ids=true | all-gather | bytes 901120 | tf_op jit(solution)/shard_map/all_gather | solution.py:54
  153.3 17.1 %all-gather.7.cloned.1.call-done = bf16[1024,2048]{1,0:T(8,128)(2,1)} async-done(((bf16[128,2048]{1,0:T(8,128)(2,1)}), bf16[1024,2048]{1,0:T(8,128)(2,1)}) %all-gather.7.cloned.1.call-update) | async-done | bytes 4194320 | tf_op jit(solution)/shard_map/all_gather | solution.py:129
  170.4 5.8 %convert_bitcast_fusion = f32[88,8,8,128]{3,1,2,0:T(8,128)S(1)} fusion(bf16[1024,2048]{1,0:T(8,128)(2,1)} %all-gather.7.cloned.1.call-done, bf16[2048,1408]{0,1:T(8,128)(2,1)} %all-gather.9.cloned.1.call-done), kind=kOutput, calls=%fused_computation.20 | convolution fusion | flops 2954231808 | bytes 9961472 | tf_op jit(solution)/shard_map/dot_general | solution.py:132
  176.2 0.7 copy.129
  176.9 5.5 %fusion.2 = f32[8,128,704]{1,0,2:T(8,128)} fusion(f32[8,128,704]{1,0,2:T(8,128)S(1)} %bitcast.73, f32[704]{0:T(1024)S(1)} %get-tuple-element.6, f32[704]{0:T(1024)S(1)} %get-tuple-element.7, f32[704]{0:T(1024)S(1)} %get-tuple-element.5), kind=kLoop, calls=%fused_computation.8 | loop fusion | flops 3604480 | bytes 5775616 | tf_op jit(solution)/shard_map/add | solution.py:69
  182.4 26.4 %all-gather.11.cloned.1.call-done = bf16[704,2048]{1,0:T(8,128)(2,1)} async-done(((bf16[704,512]{1,0:T(8,128)(2,1)}), bf16[704,2048]{1,0:T(8,128)(2,1)}) %all-gather.11.cloned.1.call-update) | async-done | bytes 2883600 | tf_op jit(solution)/shard_map/all_gather | solution.py:54
  208.8 12.9 %convolution_convert_fusion = bf16[1024,2048]{1,0:T(8,128)(2,1)} fusion(bf16[704,2048]{1,0:T(8,128)(2,1)} %all-gather.11.cloned.1.call-done, f32[88,8,8,128]{3,2,1,0:T(8,128)} %bitcast.79, bf16[1024,2048]{1,0:T(8,128)(2,1)} %all-gather.7.cloned.1.call-done, bf16[2048,1408]{0,1:T(8,128)(2,1)} %all-gather.9.cloned.1.call-done), kind=kOutput, calls=%fused_computation.4 | convolution fusion | flops 5913444352 | bytes 17039360 | tf_op jit(solution)/shard_map/dot_general | solution.py:141
  221.8 53.9 %all_to_all.21 = bf16[8,128,2048]{2,1,0:T(8,128)(2,1)S(1)} all-to-all(bf16[8,128,2048]{2,1,0:T(8,128)(2,1)} %bitcast.75), channel_id=1, replica_groups=mesh['fs_0'=4,'fs_1'=4,'tp'=8] {'tp'}, dimensions={0} | all-to-all | bytes 8388608 | tf_op jit(solution)/shard_map/all_to_all | solution.py:39
  275.7 0.7 convert_reduce_fusion
  276.4 0.9 fusion.40
  (92 shorter events, 2.0 us)
Async XLA Ops:
  6.5 44.5 %copy-start = (bf16[4,64,64]{2,1,0:T(8,128)(2,1)S(1)}, bf16[4,64,64]{2,1,0:T(8,128)(2,1)}, u32[]{:S(2)}) copy-start(bf16[4,64,64]{2,1,0:T(8,128)(2,1)} %param.18) | copy-start | bytes 98308
  6.5 13.8 %copy-start.6 = (bf16[128,704]{0,1:T(8,128)(2,1)S(1)}, bf16[128,704]{0,1:T(8,128)(2,1)}, u32[]{:S(2)}) copy-start(bf16[128,704]{0,1:T(8,128)(2,1)} %param.23) | copy-start | bytes 540676
  6.5 13.8 %copy-start.7 = (bf16[128,704]{0,1:T(8,128)(2,1)S(1)}, bf16[128,704]{0,1:T(8,128)(2,1)}, u32[]{:S(2)}) copy-start(bf16[128,704]{0,1:T(8,128)(2,1)} %param.22) | copy-start | bytes 540676
  6.5 39.2 %all-gather.5.cloned.1.call-start = ((), (), s32[]{:S(2)}) async-start(), calls=%async_computation.4 | async-start | bytes 4718592 | tf_op jit(solution)/shard_map/all_gather | solution.py:116
  7.8 13.3 %copy-start.8 = (bf16[256,128]{1,0:T(8,128)(2,1)S(1)}, bf16[256,128]{1,0:T(8,128)(2,1)}, u32[]{:S(2)}) copy-start(bf16[256,128]{1,0:T(8,128)(2,1)} %param.20) | copy-start | bytes 196612
  7.8 13.4 %copy-start.12 = (f32[256]{0:T(256)S(1)}, f32[256]{0:T(256)}, u32[]{:S(2)}) copy-start(f32[256]{0:T(256)} %param.19) | copy-start | bytes 3076
  7.9 13.4 %copy-start.11 = (f32[4,256]{1,0:T(4,128)S(1)}, f32[4,256]{1,0:T(4,128)}, u32[]{:S(2)}) copy-start(f32[4,256]{1,0:T(4,128)} %param.16) | copy-start | bytes 12292
  11.9 24.5 %all-to-all-start = ((bf16[16,128,256]{2,1,0:T(8,128)(2,1)}), bf16[16,128,256]{2,1,0:T(8,128)(2,1)S(1)}, u32[]{:S(2)}, u32[]{:S(2)}) async-start(bf16[16,128,256]{2,1,0:T(8,128)(2,1)} %broadcast_in_dim.4), calls=%async_computation | async-start | bytes 2097152 | tf_op jit(solution)/shard_map/all_to_all | solution.py:15
  20.3 133.0 %all-gather.9.cloned.1.call-start = ((), (), s32[]{:S(2)}) async-start(), calls=%async_computation.6 | async-start | bytes 6127616 | tf_op jit(solution)/shard_map/all_gather | solution.py:49
  37.4 44.2 %all-to-all-start.1 = ((bf16[16,256,128]{1,2,0:T(8,128)(2,1)}), bf16[16,256,128]{1,2,0:T(8,128)(2,1)S(1)}, u32[]{:S(2)}, u32[]{:S(2)}) async-start(bf16[16,256,128]{1,2,0:T(8,128)(2,1)} %broadcast_in_dim.5), calls=%async_computation.1 | async-start | bytes 2097152 | tf_op jit(solution)/shard_map/all_to_all | solution.py:15
  41.6 128.8 %all-gather.7.cloned.1.call-start = ((), (), s32[]{:S(2)}) async-start(), calls=%async_computation.5 | async-start | bytes 4718592 | tf_op jit(solution)/shard_map/all_gather | solution.py:129
  51.5 1.5 copy-start.13
  61.9 3.2 %copy-start.4 = (f32[8,64,256]{2,1,0:T(8,128)S(1)}, f32[8,64,256]{2,1,0:T(8,128)}, u32[]{:S(2)}) copy-start(f32[8,64,256]{2,1,0:T(8,128)} %slice.210) | copy-start | bytes 1572868
  71.6 5.0 %copy-start.3 = (f32[8,63,256]{2,1,0:T(8,128)S(1)}, f32[8,63,256]{2,1,0:T(8,128)}, u32[]{:S(2)}) copy-start(f32[8,63,256]{2,1,0:T(8,128)} %slice.205) | copy-start | bytes 1548292
  135.7 1.0 copy-start.2
  135.7 1.3 copy-start.9
  136.7 1.3 copy-start.5
  136.7 16.4 %copy-start.10 = (f32[3,704]{1,0:T(4,128)S(1)}, f32[3,704]{1,0:T(4,128)}, u32[]{:S(2)}) copy-start(f32[3,704]{1,0:T(4,128)} %param.24) | copy-start | bytes 25348
  138.0 70.8 %all-gather.11.cloned.1.call-start = ((), (), s32[]{:S(2)}) async-start(), calls=%async_computation.7 | async-start | bytes 3604480 | tf_op jit(solution)/shard_map/all_gather | solution.py:54
  221.8 55.5 %copy-start.1 = (bf16[4,64,64]{2,1,0:T(8,128)(2,1)S(1)}, bf16[4,64,64]{2,1,0:T(8,128)(2,1)}, u32[]{:S(2)}) copy-start(bf16[4,64,64]{2,1,0:T(8,128)(2,1)} %param.18) | copy-start | bytes 98308
Sparse Core Ops, SparseCore 0:
  10.1 35.6 all-gather.4
  47.9 62.6 all-gather.8
  138.1 32.2 all-gather.6
  171.9 36.8 all-gather.10
where the time goes:
time: 285 us; the launch traced here: 284 us
  blocking collectives  121 us (42%)
  waiting for transfers between devices  62.8 us (22%)
  matrix products  25.5 us (9%)
  local copies, waits for them, and re-layouts  25.3 us (9%)
  other arithmetic  22.9 us (8%)
  between operations  13.8 us (5%)
  starting transfers between devices  12.7 us (4%)
    all_to_all x2, blocking collectives, sent_and_summed(): pieces = lax.all_to_all(in_blocks(shard, dim, size), axis, 0, 0, tiled=True)  106 us
    all_gather x1, waiting for transfers between devices, gathered_by_axis(): shard = lax.all_gather(shard, axis, axis=dim, tiled=True)  26.4 us
    all_gather x1, waiting for transfers between devices, shards(): gathered_two = lax.all_gather(normed_two, 'tp', axis=0, tiled=True)  17.1 us
    all_gather x1, blocking collectives, gathered_by_axis(): shard = lax.all_gather(shard, axis, axis=dim, tiled=True)  15.1 us
    all_to_all x2, waiting for transfers between devices, copy_for_each(): lax.all_to_all(jnp.broadcast_to(shard[None], (size, *shard.shape)), axis,...  15 us
    dot_general x1, matrix products, shards(): jnp.dot(hidden, gathered_by_axis(down_weight, FS, 1), preferred_element_t...  12.9 us
    all_to_all x2, starting transfers between devices, copy_for_each(): lax.all_to_all(jnp.broadcast_to(shard[None], (size, *shard.shape)), axis,...  12.6 us
    slice x39, local copies, waits for them, and re-layouts, recurrence(): state = lax.associative_scan(combine, (decay, drive), axis=1)[1]  10.3 us
  transfers between devices with their start and end apart: 6, of which 4 were waited for; matrix products, arithmetic and copies ran while one was open for 20% of the time, Pallas kernels for 0%

commit v1 on v0

v1 whole, which is shorter than its diff:
```python
import jax
import jax.numpy as jnp
from jax import lax
from jax.experimental import pallas as pl
from jax.experimental.pallas import tpu as pltpu
from jax.sharding import Mesh
from jax.sharding import PartitionSpec as P

GATE_BLOCK = 64
SEQ = 128
HALF = 64
RING = 4
MESH = pl.DeviceIdType.MESH
BF16 = jnp.bfloat16
F32 = jnp.float32

OWN, RIGHT, LEFT, FAR, IN_RIGHT, IN_LEFT, IN_FAR = 0, 2, 4, 6, 8, 10, 12


def remote(src, dst, send_sem, recv_sem, **device):
    return pltpu.make_async_remote_copy(
        src_ref=src,
        dst_ref=dst,
        send_sem=send_sem,
        recv_sem=recv_sem,
        device_id=device,
        device_id_type=MESH,
    )


def far_order(k):
    return lax.rem(k * (k + 1) // 2, RING)


def rms_rows(wide, gain):
    scale = lax.rsqrt(jnp.mean(wide * wide, axis=-1, keepdims=True) + 1e-06)
    return (wide * scale * gain).astype(BF16)


def shifted(values, rows, by, fill):
    return jnp.where(rows >= by, pltpu.roll(values, by, axis=0), fill)


def kernel(
    resid,
    mix_gain,
    in_w,
    conv_taps,
    recur_w,
    input_w,
    decay_rate,
    out_w,
    mlp_gain,
    up_w,
    ffn_taps,
    down_w,
    result,
    in_g,
    out_g,
    up_g,
    down_g,
    rows_g,
    gate_w,
    proj,
    gates,
    recurred,
    pre,
    hidden,
    partial,
    from_core,
    to_ring,
    far_in,
    near_in,
    middle,
    w_send,
    w_recv,
    w_local,
    g_send,
    g_recv,
    c_send,
    c_recv,
    r_send,
    r_recv,
):
    z, x, y, c = (lax.axis_index(a) for a in ("z", "x", "y", "c"))
    at = {"z": z, "x": x, "y": y}

    def nxt(axis, by):
        return lax.rem(at[axis] + (by + RING), RING)

    other = 1 - c
    y_right, y_left, y_far = nxt("y", 1), nxt("y", -1), nxt("y", 2)

    barrier = pltpu.get_barrier_semaphore()
    for axis in ("z", "x", "y"):
        for by in (1, -1):
            pl.semaphore_signal(
                barrier, inc=1, device_id={axis: nxt(axis, by)}, device_id_type=MESH
            )
    pl.semaphore_signal(barrier, inc=1, device_id={"c": other}, device_id_type=MESH)
    pl.semaphore_wait(barrier, 7)

    weights = ((in_w, in_g), (out_w, out_g), (up_w, up_g), (down_w, down_g))

    def piece(i, p):
        rows = weights[i][1].shape[2] // 4
        return pl.ds(p * rows, rows)

    def axes_of(p):
        return ("x", "z") if p < 2 else ("z", "x")

    def slot(i, p, axis, by):
        g = weights[i][1]
        if axis == "x":
            return g.at[z, nxt("x", by), piece(i, p)]
        return g.at[nxt("z", by), x, piece(i, p)]

    def line(i, p, axis, by):
        g = weights[i][1]
        if axis == "z":
            return g.at[nxt("z", by), :, piece(i, p)]
        return g.at[:, nxt("x", by), piece(i, p)]

    def w_copy(i, p, src, dst, k, axis, by):
        return remote(src, dst, w_send.at[i, p, k], w_recv.at[i, p, k], **{axis: nxt(axis, by)})

    def own_copy(i):
        src, g = weights[i]
        return pltpu.make_async_copy(src, g.at[z, x], w_local.at[i])

    def first_send(i):
        src = weights[i][0]
        for p in range(4):
            axis = axes_of(p)[0]
            for k, by in ((0, 1), (1, -1)):
                w_copy(i, p, src.at[piece(i, p)], slot(i, p, axis, 0), k, axis, by).start()

    def first_wait(i, p, k):
        axis = axes_of(p)[0]
        by = (-1, 1, 2)[k]
        there = slot(i, p, axis, by)
        w_copy(i, p, there, there, k, axis, 1).wait_recv()

    def first_forward(i):
        for p in range(4):
            axis = axes_of(p)[0]
            k = p % 2
            first_wait(i, p, k)
            by = 1 if k == 0 else -1
            there = slot(i, p, axis, -by)
            w_copy(i, p, there, there, 2, axis, by).start()

    def second_send(i):
        own_copy(i).wait()
        for p in range(4):
            axis = axes_of(p)[1]
            first_wait(i, p, 1 - p % 2)
            first_wait(i, p, 2)
            here = line(i, p, axis, 0)
            for k, by in ((3, 1), (4, -1)):
                w_copy(i, p, here, here, k, axis, by).start()

    def second_wait(i, p, k):
        axis = axes_of(p)[1]
        by = (-1, 1, 2)[k - 3]
        there = line(i, p, axis, by)
        w_copy(i, p, there, there, k, axis, 1).wait_recv()

    def second_forward(i):
        for p in range(4):
            axis = axes_of(p)[1]
            k = 3 + p % 2
            second_wait(i, p, k)
            by = 1 if k == 3 else -1
            there = line(i, p, axis, -by)
            w_copy(i, p, there, there, 5, axis, by).start()

    def weights_done(i):
        for p in range(4):
            second_wait(i, p, 4 - p % 2)
            second_wait(i, p, 5)

    def weights_sent(i):
        for p in range(4):
            first, second = axes_of(p)
            one, four = slot(i, p, first, 0), line(i, p, second, 0)
            for k in range(6):
                ref = one if k < 3 else four
                w_copy(i, p, ref, ref, k, first, 1).wait_send()

    def g_copy(n, yq, cq, h, s, r, **device):
        ref = rows_g.at[n, yq, cq, h]
        return remote(ref, ref, g_send.at[n, s], g_recv.at[n, r], **device)

    def rows_wait(n, yq, cq, h, r):
        g_copy(n, yq, cq, h, 0, r, c=other).wait_recv()

    def rows_send(n):
        for h in (0, 1):
            g_copy(n, y, c, h, h, IN_LEFT + h, y=y_right).start()
            g_copy(n, y, c, 1 - h, 2 + 1 - h, IN_RIGHT + 1 - h, y=y_left).start()
            g_copy(n, y, c, h, 4 + h, OWN + h, c=other).start()

    def rows_first(n):
        rows_wait(n, y_left, c, 0, IN_LEFT)
        g_copy(n, y_left, c, 0, 6, IN_FAR, y=y_right).start()
        g_copy(n, y_left, c, 0, 8, LEFT, c=other).start()
        rows_wait(n, y_right, c, 1, IN_RIGHT + 1)
        g_copy(n, y_right, c, 1, 7, IN_FAR + 1, y=y_left).start()
        g_copy(n, y_right, c, 1, 11, RIGHT + 1, c=other).start()

    def rows_second(n):
        rows_wait(n, y_left, c, 1, IN_LEFT + 1)
        g_copy(n, y_left, c, 1, 9, LEFT + 1, c=other).start()
        rows_wait(n, y_right, c, 0, IN_RIGHT)
        g_copy(n, y_right, c, 0, 10, RIGHT, c=other).start()

    def rows_third(n):
        for h in (0, 1):
            rows_wait(n, y_far, c, h, IN_FAR + h)
            g_copy(n, y_far, c, h, 12 + h, FAR + h, c=other).start()

    def rows_sent(n):
        for s in range(14):
            g_copy(n, y, c, 0, s, 0, c=other).wait_send()

    def pair_ready(n, k, yq):
        for h in (0, 1):
            rows_wait(n, yq, other, h, 2 * k + h)

    def core_copy(n, yq, k):
        return remote(
            partial.at[yq, other], from_core.at[n, yq], c_send.at[n, k], c_recv.at[n, k], c=other
        )

    def r_copy(n, src, dst, k, **device):
        return remote(src, dst, r_send.at[n, k], r_recv.at[n, k], **device)

    def chip_sum(n, yq, h, at_row, extra=None):
        rows = pl.ds(h * HALF + at_row, 16)
        total = partial[yq, c, rows, :].astype(F32) + from_core[n, yq, rows, :].astype(F32)
        if extra is not None:
            total = total + extra[pl.ds(at_row, 16), :].astype(F32)
        return total

    def fill_ring(n, j, h, yq, extra=None):
        @pl.loop(0, HALF, step=16)
        def _(at_row):
            at_row = pl.multiple_of(at_row, 16)
            to_ring[n, j, h, pl.ds(at_row, 16), :] = chip_sum(n, yq, h, at_row, extra).astype(BF16)

    def sums_far(n):
        core_copy(n, y_far, 0).wait_recv()
        fill_ring(n, 0, 0, y_far)
        r_copy(n, to_ring.at[n, 0, 0], far_in.at[n, 0], 0, y=y_right).start()
        fill_ring(n, 0, 1, y_far)
        r_copy(n, to_ring.at[n, 0, 1], far_in.at[n, 1], 1, y=y_left).start()

    def sums_left(n):
        core_copy(n, y_left, 1).wait_recv()
        fill_ring(n, 1, 0, y_left)
        r_copy(n, to_ring.at[n, 1, 0], near_in.at[n, 1, 0], 2, y=y_left).start()

    def sums_right(n):
        core_copy(n, y_right, 2).wait_recv()
        fill_ring(n, 2, 1, y_right)
        r_copy(n, to_ring.at[n, 2, 1], near_in.at[n, 0, 1], 3, y=y_right).start()

    def sums_near(n):
        r_copy(n, far_in.at[n, 0], far_in.at[n, 0], 0, y=y_right).wait_recv()
        fill_ring(n, 2, 0, y_right, far_in.at[n, 0])
        r_copy(n, to_ring.at[n, 2, 0], near_in.at[n, 0, 0], 4, y=y_right).start()
        r_copy(n, far_in.at[n, 1], far_in.at[n, 1], 1, y=y_right).wait_recv()
        fill_ring(n, 1, 1, y_left, far_in.at[n, 1])
        r_copy(n, to_ring.at[n, 1, 1], near_in.at[n, 1, 1], 5, y=y_left).start()

    def near_wait(n, side, h):
        k = ((4, 3), (2, 5))[side][h]
        ref = near_in.at[n, side, h]
        r_copy(n, ref, ref, k, y=y_right).wait_recv()

    def sums_sent(n):
        for k in range(4):
            core_copy(n, y, k).wait_send()
        for k in range(6):
            r_copy(n, to_ring.at[n, 0, 0], to_ring.at[n, 0, 0], k, y=y_right).wait_send()

    def sums_wait(n):
        core_copy(n, y, 3).wait_recv()
        for side in (0, 1):
            for h in (0, 1):
                near_wait(n, side, h)

    def own_sum(n, h, at_row):
        total = chip_sum(n, y, h, at_row)
        for side in (0, 1):
            total = total + near_in[n, side, h, pl.ds(at_row, 16), :].astype(F32)
        return total

    for i in range(4):
        own_copy(i).start()
    first_send(0)
    first_send(1)

    for h in (0, 1):

        @pl.loop(0, HALF, step=16)
        def _(at_row):
            at_row = pl.multiple_of(at_row, 16)
            wide = resid[pl.ds(h * HALF + at_row, 16), :].astype(F32)
            rows_g[0, y, c, h, pl.ds(at_row, 16), :] = rms_rows(wide, mix_gain[...])

    rows_send(0)

    gate_w[...] = jnp.zeros_like(gate_w)
    for n in range(recur_w.shape[0]):
        block = slice(n * GATE_BLOCK, (n + 1) * GATE_BLOCK)
        gate_w[block, block] = recur_w[n]
        block_two = slice(256 + n * GATE_BLOCK, 256 + (n + 1) * GATE_BLOCK)
        gate_w[block, block_two] = input_w[n]

    first_forward(0)
    first_forward(1)
    second_send(0)
    second_send(1)
    first_send(2)
    first_send(3)
    rows_first(0)
    second_forward(0)
    second_forward(1)
    rows_second(0)
    first_forward(2)
    first_forward(3)
    weights_done(0)

    @pl.loop(0, RING)
    def _(k):
        @pl.when(k == 2)
        def _():
            second_send(2)

        @pl.when(k == 3)
        def _():
            rows_third(0)

        yq = lax.rem(y + far_order(k), RING)
        pair_ready(0, k, yq)
        columns = rows_g[0, yq].reshape(2 * SEQ, -1)
        w = in_g[...].reshape(-1, 256)
        wide = jnp.dot(columns, w, preferred_element_type=F32)
        wide = wide.astype(BF16).astype(F32)
        rows2 = lax.rem(lax.broadcasted_iota(jnp.int32, wide.shape, 0), SEQ)
        taps = conv_taps[...]
        conv = shifted(wide, rows2, 3, 0.0) * taps[0:1]
        conv = conv + shifted(wide, rows2, 2, 0.0) * taps[1:2]
        conv = conv + shifted(wide, rows2, 1, 0.0) * taps[2:3]
        conv = conv + wide * taps[3:4]
        proj[...] = conv
        gates[...] = jnp.dot(conv.astype(BF16), gate_w[...], preferred_element_type=F32)

        for s in range(2):
            for b in range(2):
                rows = slice(s * SEQ, (s + 1) * SEQ)
                lanes = slice(b * 128, (b + 1) * 128)
                lanes2 = slice(256 + b * 128, 256 + (b + 1) * 128)
                rgate = jax.nn.sigmoid(gates[rows, lanes])
                igate = jax.nn.sigmoid(gates[rows, lanes2])
                a = 8.0 * rgate * decay_rate[:, lanes]
                decay = jnp.exp(-a)
                a2 = a * a
                small = 2.0 * decay * (a * (1.0 + a2 * (1.0 / 6) * (1.0 + a2 * (1.0 / 20) * (1.0 + a2 * (1.0 / 42)))))
                left_over = jnp.where(a < 0.3, small, 1.0 - decay * decay)
                state = jnp.sqrt(left_over) * (igate * proj[rows, lanes])
                pos = lax.broadcasted_iota(jnp.int32, state.shape, 0)
                by = 1
                while by < SEQ:
                    state = decay * shifted(state, pos, by, 0.0) + state
                    if 2 * by < SEQ:
                        decay = decay * shifted(decay, pos, by, 1.0)
                    by *= 2
                recurred[yq, rows, lanes] = state.astype(BF16)

    weights_done(1)
    second_send(3)

    def mixed(yq):
        left = recurred[yq]
        for zq in range(RING):
            w = jnp.concatenate([out_g[zq, xq] for xq in range(RING)], axis=1)
            term = jnp.dot(left, w, preferred_element_type=F32).astype(BF16)
            for s in range(2):
                partial[yq, s, :, zq * 512 : (zq + 1) * 512] = term[s * SEQ : (s + 1) * SEQ]

    def lowered(yq):
        left = hidden[yq]
        for zq in range(RING):
            w = jnp.concatenate([down_g[zq, xq] for xq in range(RING)], axis=1)
            term = jnp.dot(left, w, preferred_element_type=F32).astype(BF16)
            for s in range(2):
                partial[yq, s, :, zq * 512 : (zq + 1) * 512] = term[s * SEQ : (s + 1) * SEQ]

    def summed(n, product):
        @pl.loop(0, RING)
        def _(k):
            yq = lax.rem(y + far_order(RING - 1 - k), RING)
            product(yq)
            core_copy(n, yq, k).start()
            for step, part in ((1, sums_far), (2, sums_left), (3, sums_right)):

                @pl.when(k == step)
                def _():
                    part(n)

        sums_near(n)

    summed(0, mixed)
    second_forward(2)
    sums_wait(0)

    for h in (0, 1):

        @pl.loop(0, HALF, step=16)
        def _(at_row):
            at_row = pl.multiple_of(at_row, 16)
            here = pl.ds(h * HALF + at_row, 16)
            mid = (resid[here, :].astype(F32) + own_sum(0, h, at_row)).astype(BF16)
            middle[here, :] = mid
            rows_g[1, y, c, h, pl.ds(at_row, 16), :] = rms_rows(mid.astype(F32), mlp_gain[...])

    rows_send(1)
    sums_sent(0)
    weights_done(2)

    def gated(gate, value, taps, pos):
        conv = shifted(gate, pos, 2, 0.0) * taps[0:1]
        conv = conv + shifted(gate, pos, 1, 0.0) * taps[1:2]
        conv = conv + gate * taps[2:3]
        return (conv / (1.0 + jnp.exp(-conv)) * value).astype(BF16)

    @pl.loop(0, RING)
    def _(k):
        @pl.when(k == 1)
        def _():
            rows_first(1)
            rows_second(1)

        @pl.when(k == 2)
        def _():
            second_forward(3)

        @pl.when(k == 3)
        def _():
            rows_third(1)

        yq = lax.rem(y + far_order(k), RING)
        pair_ready(1, k, yq)
        columns = rows_g[1, yq].reshape(2 * SEQ, -1)
        w = up_g[...].reshape(-1, 1408)
        pre[...] = jnp.dot(columns, w, preferred_element_type=F32)

        for s in range(2):
            rows = slice(s * SEQ, (s + 1) * SEQ)
            for b in range(6):
                lanes = slice(b * 128, (b + 1) * 128)
                if b < 5:
                    gate = pre[rows, lanes].astype(BF16).astype(F32)
                    value = pre[rows, 640 + b * 128 : 640 + (b + 1) * 128].astype(BF16).astype(F32)
                else:
                    gate = pre[rows, 1280:1408].astype(BF16).astype(F32)
                    value = pltpu.roll(gate, 64, axis=1)
                pos = lax.broadcasted_iota(jnp.int32, gate.shape, 0)
                unit = gated(gate, value, ffn_taps[:, lanes], pos)
                if b < 5:
                    hidden[yq, rows, lanes] = unit
                else:
                    hidden[yq, rows, 640:704] = unit[:, :64]

    weights_done(3)
    summed(1, lowered)
    sums_wait(1)

    for h in (0, 1):

        @pl.loop(0, HALF, step=16)
        def _(at_row):
            at_row = pl.multiple_of(at_row, 16)
            here = pl.ds(h * HALF + at_row, 16)
            result[here, :] = (middle[here, :].astype(F32) + own_sum(1, h, at_row)).astype(BF16)

    sums_sent(1)
    for n in range(2):
        rows_sent(n)
    for i in range(4):
        weights_sent(i)


def shards(
    resid,
    mix_gain,
    in_weight,
    conv_taps,
    recur_gate_w,
    input_gate_w,
    decay_rate,
    out_weight,
    mlp_gain,
    up_gate_w,
    up_val_w,
    ffn_taps,
    down_weight,
):
    up = jnp.concatenate(
        [up_gate_w[:, :640], up_val_w[:, :640], up_gate_w[:, 640:], up_val_w[:, 640:]], axis=1
    )
    taps = jnp.pad(ffn_taps, ((0, 0), (0, 64)))
    vmem = pl.BlockSpec(memory_space=pltpu.VMEM)
    hbm = pl.BlockSpec(memory_space=pl.ANY)
    dma = pltpu.SemaphoreType.DMA
    width = resid.shape[1]
    return pl.pallas_call(
        kernel,
        name="layer",
        out_shape=jax.ShapeDtypeStruct(resid.shape, BF16),
        in_specs=[vmem, vmem, hbm, vmem, vmem, vmem, vmem, hbm, vmem, hbm, vmem, hbm],
        out_specs=vmem,
        scratch_shapes=[
            pltpu.VMEM((RING, RING, *in_weight.shape), BF16),
            pltpu.VMEM((RING, RING, *out_weight.shape), BF16),
            pltpu.VMEM((RING, RING, *up.shape), BF16),
            pltpu.VMEM((RING, RING, *down_weight.shape), BF16),
            pltpu.VMEM((2, RING, 2, 2, HALF, width), BF16),
            pltpu.VMEM((256, 512), BF16),
            pltpu.VMEM((2 * SEQ, 256), F32),
            pltpu.VMEM((2 * SEQ, 512), F32),
            pltpu.VMEM((RING, 2 * SEQ, 256), BF16),
            pltpu.VMEM((2 * SEQ, up.shape[1]), F32),
            pltpu.VMEM((RING, 2 * SEQ, 704), BF16),
            pltpu.VMEM((RING, 2, SEQ, width), BF16),
            pltpu.VMEM((2, RING, SEQ, width), BF16),
            pltpu.VMEM((2, 3, 2, HALF, width), BF16),
            pltpu.VMEM((2, 2, HALF, width), BF16),
            pltpu.VMEM((2, 2, 2, HALF, width), BF16),
            pltpu.VMEM((SEQ, width), BF16),
            dma((4, 4, 6)),
            dma((4, 4, 6)),
            dma((4,)),
            dma((2, 14)),
            dma((2, 14)),
            dma((2, 4)),
            dma((2, 4)),
            dma((2, 6)),
            dma((2, 6)),
        ],
        compiler_params=pltpu.CompilerParams(
            collective_id=0, has_side_effects=True, vmem_limit_bytes=60 * 1024 * 1024
        ),
    )(
        resid,
        mix_gain[None],
        in_weight,
        conv_taps,
        recur_gate_w,
        input_gate_w,
        decay_rate[None],
        out_weight,
        mlp_gain[None],
        up,
        taps,
        down_weight,
    )


def solution(mesh):
    split = Mesh(mesh.devices.reshape(RING, RING, RING, 2), ("z", "x", "y", "c"))
    fs, tp = ("z", "x"), ("y", "c")
    rows = ("z", "x", "y", "c")
    return jax.shard_map(
        shards,
        mesh=split,
        in_specs=(
            P(rows, None),
            P(),
            P(fs, tp),
            P(None, tp),
            P(tp, None, None),
            P(tp, None, None),
            P(tp),
            P(tp, fs),
            P(),
            P(fs, tp),
            P(fs, tp),
            P(None, tp),
            P(tp, fs),
        ),
        out_specs=P(rows, None),
        check_vma=False,
    )
```

time: 285 us -> 118 us (0.41)
  blocking collectives: 121 us -> 0 us
  Pallas kernels: 0 us -> 110 us
  waiting for transfers between devices: 62.8 us -> 0 us
  matrix products: 25.5 us -> 0 us
  other arithmetic: 22.9 us -> 0 us
  local copies, waits for them, and re-layouts: 25.3 us -> 7.83 us
  between operations: 13.8 us -> 0.04 us
  starting transfers between devices: 12.7 us -> 0 us
    pallas_call x0 -> x1, Pallas kernels: none -> 110 us  [shards(): pl.pallas_call(kernel, name='layer', out_shape=jax.ShapeDtypeStruct(resid...]
    all_to_all x2 -> x0, blocking collectives: 106 us -> none  [sent_and_summed(): pieces = lax.all_to_all(in_blocks(shard, dim, size), axis, 0, 0, tiled=True)]
    all_gather x4 -> x0, waiting for transfers between devices: 47.7 us -> none  [the longest x1 26.4 us: gathered_by_axis(): shard = lax.all_gather(shard, axis, axis=dim, tiled=True)]
    dot_general x6 -> x0, matrix products: 25.5 us -> none  [the longest x1 12.9 us: shards(): jnp.dot(hidden, gathered_by_axis(down_weight, FS, 1), preferred_element_t...]
    all_gather x1 -> x0, blocking collectives: 15.1 us -> none  [gathered_by_axis(): shard = lax.all_gather(shard, axis, axis=dim, tiled=True)]
    all_to_all x2 -> x0, waiting for transfers between devices: 15 us -> none  [copy_for_each(): lax.all_to_all(jnp.broadcast_to(shard[None], (size, *shard.shape)), axis,...]
    all_to_all x2 -> x0, starting transfers between devices: 12.6 us -> none  [copy_for_each(): lax.all_to_all(jnp.broadcast_to(shard[None], (size, *shard.shape)), axis,...]
    add x14 -> x0, other arithmetic: 7.48 us -> none  [the longest x1 5.48 us: causal_taps(): summed + padded[:, tap_index:tap_index + length] * tap_weights[tap_index]]
  transfers between devices with their start and end apart: 6 -> 0, of which waited for: 4 -> 0; matrix products, arithmetic and copies ran while one was open for 20% -> 0% of each run, Pallas kernels for 0% -> 0%
where the time goes in v1:
time: 118 us; the launch traced here: 117 us
  Pallas kernels  110 us (93%)
  local copies, waits for them, and re-layouts  7.83 us (7%)
    pallas_call x1, Pallas kernels, shards(): pl.pallas_call(kernel, name='layer', out_shape=jax.ShapeDtypeStruct(resid...  110 us
    unnamed x5, local copies, waits for them, and re-layouts  2.43 us

profile of v1, /device:TPU:1, one launch (start us, length us, event | category | flops | bytes accessed | tf_op | source)
XLA Modules:
  0.0 117.5 jit_solution(17328244902096775753)
XLA Ops:
  0.0 1.3 %pad.4.ffn_taps = f32[3,768]{1,0:T(4,128)} pad(f32[3,704]{1,0:T(4,128)} %param.24, f32[]{:T(128)} %constant.2.clone.1), padding=0_0x0_64 | pad | bytes 17668 | tf_op jit(solution)/shard_map/jit(_pad)/pad | solution.py:515
  1.3 0.0 slice-start
  1.3 0.7 slice-done
  2.0 0.1 copy.20
  2.1 0.0 slice-start.2
  2.2 0.7 slice-done.2
  2.9 0.1 copy.21
  3.0 0.0 slice-start.1
  3.0 0.9 slice-done.1
  3.9 0.2 copy.18
  4.1 0.0 slice-start.3
  4.1 0.9 slice-done.3
  5.0 0.2 copy.19
  5.2 0.8 concatenate.3.up_w
  6.0 109.6 %layer.1 = bf16[128,2048]{1,0:T(8,128)(2,1)} custom-call(bf16[128,2048]{1,0:T(8,128)(2,1)} %resid.1, f32[1,2048]{1,0:T(1,128)} %bitcast.3, bf16[128,256]{1,0:T(8,128)(2,1)} %in_w.1, f32[4,256]{1,0:T(4,128)} %conv_taps.1, bf16[4,64,64]{2,1,0:T(8,128)(2,1)} %recur_w.1, bf16[4,64,64]{2,1,0:T(8,128)(2,1)} %input_w.1, f32[1,256]{1,0:T(1,128)} %bitcast.5, ...), custom_call_target="tpu_custom_call" | custom-call | tf_op jit(solution)/shard_map/layer/pallas_call | solution.py:520
  115.6 1.9 %copy.23 = bf16[128,2048]{1,0:T(8,128)(2,1)} copy(bf16[128,2048]{1,0:T(8,128)(2,1)} %layer.1) | data formatting | bytes 1048576
Async XLA Ops:
  1.3 0.7 slice-start
  2.1 0.7 slice-start.2
  3.0 0.9 slice-start.1
  4.1 0.9 slice-start.3

commit v2 on v1

v2 whole, which is shorter than its diff:
```python
import jax
import jax.numpy as jnp
from jax import lax
from jax.experimental import pallas as pl
from jax.experimental.pallas import tpu as pltpu
from jax.sharding import Mesh
from jax.sharding import PartitionSpec as P

GATE_BLOCK = 64
SEQ = 128
HALF = 64
QUARTER = 32
RING = 4
MESH = pl.DeviceIdType.MESH
BF16 = jnp.bfloat16
F32 = jnp.float32

OWN, RIGHT, LEFT, FAR, IN_RIGHT, IN_LEFT, IN_FAR = 0, 2, 4, 6, 8, 10, 12


def remote(src, dst, send_sem, recv_sem, **device):
    return pltpu.make_async_remote_copy(
        src_ref=src,
        dst_ref=dst,
        send_sem=send_sem,
        recv_sem=recv_sem,
        device_id=device,
        device_id_type=MESH,
    )


def rms_rows(wide, gain):
    scale = lax.rsqrt(jnp.mean(wide * wide, axis=-1, keepdims=True) + 1e-06)
    return (wide * scale * gain).astype(BF16)


def shifted(values, rows, by, fill):
    return jnp.where(rows >= by, pltpu.roll(values, by, axis=0), fill)


def behind(extended, by):
    return pltpu.roll(extended, by, axis=0)[8:]


def kernel(
    resid_hbm,
    mix_gain,
    in_w,
    conv_taps,
    recur_w,
    input_w,
    decay_rate,
    out_w,
    mlp_gain,
    gate_t,
    value_t,
    ffn_taps,
    down_w,
    result,
    resid,
    gate_in,
    value_in,
    in_g,
    out_g,
    up_g,
    down_g,
    rows_g,
    gate_w,
    proj,
    gates,
    conv_tail,
    carry,
    recurred,
    pre,
    gate_tail,
    hidden,
    partial,
    from_core,
    to_ring,
    far_in,
    near_in,
    middle,
    w_send,
    w_recv,
    l_sem,
    g_send,
    g_recv,
    c_send,
    c_recv,
    r_send,
    r_recv,
):
    z, x, y, c = (lax.axis_index(a) for a in ("z", "x", "y", "c"))
    at = {"z": z, "x": x, "y": y}

    def nxt(axis, by):
        return lax.rem(at[axis] + (by + RING), RING)

    other = 1 - c
    y_right, y_left, y_far = nxt("y", 1), nxt("y", -1), nxt("y", 2)

    weights = ((in_w, in_g), (out_w, out_g), (None, up_g), (down_w, down_g))

    def own_copy(i):
        if i < 4:
            src, g = weights[i]
            return pltpu.make_async_copy(src, g.at[z, x], l_sem.at[i])
        src, dst = ((resid_hbm, resid), (gate_t, gate_in), (value_t, value_in))[i - 4]
        return pltpu.make_async_copy(src, dst, l_sem.at[i])

    for i in (4, 5, 6, 0, 1, 3):
        own_copy(i).start()

    barrier = pltpu.get_barrier_semaphore()
    for axis in ("z", "x", "y"):
        for by in (1, -1):
            pl.semaphore_signal(
                barrier, inc=1, device_id={axis: nxt(axis, by)}, device_id_type=MESH
            )
    pl.semaphore_signal(barrier, inc=1, device_id={"c": other}, device_id_type=MESH)
    pl.semaphore_wait(barrier, 7)

    def piece(i, p):
        rows = weights[i][1].shape[2] // 4
        return pl.ds(p * rows, rows)

    def axes_of(p):
        return ("x", "z") if p < 2 else ("z", "x")

    def slot(i, p, axis, by):
        g = weights[i][1]
        if axis == "x":
            return g.at[z, nxt("x", by), piece(i, p)]
        return g.at[nxt("z", by), x, piece(i, p)]

    def line(i, p, axis, by):
        g = weights[i][1]
        if axis == "z":
            return g.at[nxt("z", by), :, piece(i, p)]
        return g.at[:, nxt("x", by), piece(i, p)]

    def w_copy(i, p, src, dst, k, axis, by):
        return remote(src, dst, w_send.at[i, p, k], w_recv.at[i, p, k], **{axis: nxt(axis, by)})

    def first_send(i):
        src = weights[i][0]
        for p in range(4):
            axis = axes_of(p)[0]
            here = slot(i, p, axis, 0)
            for k, by in ((0, 1), (1, -1)):
                w_copy(i, p, here if src is None else src.at[piece(i, p)], here, k, axis, by).start()

    def first_wait(i, p, k):
        axis = axes_of(p)[0]
        there = slot(i, p, axis, (-1, 1, 2)[k])
        w_copy(i, p, there, there, k, axis, 1).wait_recv()

    def first_forward(i):
        for p in range(4):
            axis = axes_of(p)[0]
            k = p % 2
            first_wait(i, p, k)
            by = 1 if k == 0 else -1
            there = slot(i, p, axis, -by)
            w_copy(i, p, there, there, 2, axis, by).start()

    def second_send(i):
        if weights[i][0] is not None:
            own_copy(i).wait()
        for p in range(4):
            axis = axes_of(p)[1]
            first_wait(i, p, 1 - p % 2)
            first_wait(i, p, 2)
            here = line(i, p, axis, 0)
            for k, by in ((3, 1), (4, -1)):
                w_copy(i, p, here, here, k, axis, by).start()

    def second_wait(i, p, k):
        axis = axes_of(p)[1]
        there = line(i, p, axis, (-1, 1, 2)[k - 3])
        w_copy(i, p, there, there, k, axis, 1).wait_recv()

    def second_forward(i):
        for p in range(4):
            axis = axes_of(p)[1]
            k = 3 + p % 2
            second_wait(i, p, k)
            by = 1 if k == 3 else -1
            there = line(i, p, axis, -by)
            w_copy(i, p, there, there, 5, axis, by).start()

    def weights_done(i):
        for p in range(4):
            second_wait(i, p, 4 - p % 2)
            second_wait(i, p, 5)

    def weights_sent(i):
        for p in range(4):
            first, second = axes_of(p)
            one, four = slot(i, p, first, 0), line(i, p, second, 0)
            for k in range(6):
                ref = one if k < 3 else four
                w_copy(i, p, ref, ref, k, first, 1).wait_send()

    def g_copy(n, yq, cq, q, s, r, **device):
        ref = rows_g.at[n, yq, cq, q]
        return remote(ref, ref, g_send.at[n, s], g_recv.at[n, r], **device)

    def rows_wait(n, yq, cq, q, r):
        g_copy(n, yq, cq, q, 0, r, c=other).wait_recv()

    def rows_send(n):
        for q in (0, 1):
            g_copy(n, y, c, q, q, IN_LEFT + q, y=y_right).start()
            g_copy(n, y, c, 1 - q, 2 + 1 - q, IN_RIGHT + 1 - q, y=y_left).start()
            g_copy(n, y, c, q, 4 + q, OWN + q, c=other).start()

    def rows_first(n):
        rows_wait(n, y_left, c, 0, IN_LEFT)
        g_copy(n, y_left, c, 0, 6, IN_FAR, y=y_right).start()
        g_copy(n, y_left, c, 0, 8, LEFT, c=other).start()
        rows_wait(n, y_right, c, 1, IN_RIGHT + 1)
        g_copy(n, y_right, c, 1, 7, IN_FAR + 1, y=y_left).start()
        g_copy(n, y_right, c, 1, 11, RIGHT + 1, c=other).start()

    def rows_second(n):
        rows_wait(n, y_left, c, 1, IN_LEFT + 1)
        g_copy(n, y_left, c, 1, 9, LEFT + 1, c=other).start()
        rows_wait(n, y_right, c, 0, IN_RIGHT)
        g_copy(n, y_right, c, 0, 10, RIGHT, c=other).start()

    def rows_third(n):
        for q in (0, 1):
            rows_wait(n, y_far, c, q, IN_FAR + q)
            g_copy(n, y_far, c, q, 12 + q, FAR + q, c=other).start()

    def rows_sent(n):
        for s in range(14):
            g_copy(n, y, c, 0, s, 0, c=other).wait_send()

    def group(g):
        return (y, y_right) if g == 0 else (y_left, y_far)

    def group_rows(n, g):
        for j, yq in enumerate(group(g)):
            for q in (0, 1):
                rows_wait(n, yq, other, q, 4 * g + 2 * j + q)
        return jnp.concatenate([rows_g[n, yq].reshape(2 * HALF, -1) for yq in group(g)], axis=0)

    def core_copy(n, yq, k):
        return remote(
            partial.at[n, yq, other], from_core.at[n, yq], c_send.at[n, k], c_recv.at[n, k], c=other
        )

    def r_copy(n, src, dst, k, **device):
        return remote(src, dst, r_send.at[n, k], r_recv.at[n, k], **device)

    def chip_sum(n, yq, at_row):
        rows = pl.ds(at_row, 16)
        return partial[n, yq, c, rows, :].astype(F32) + from_core[n, yq, rows, :].astype(F32)

    def fill_ring(n, j, q, yq, extra=None):
        for at_row in range(0, QUARTER, 16):
            total = chip_sum(n, yq, q * QUARTER + at_row)
            if extra is not None:
                total = total + extra[at_row : at_row + 16, :].astype(F32)
            to_ring[n, j, q, at_row : at_row + 16, :] = total.astype(BF16)

    def sums_far(n):
        core_copy(n, y_far, 0).wait_recv()
        fill_ring(n, 0, 0, y_far)
        r_copy(n, to_ring.at[n, 0, 0], far_in.at[n, 0], 0, y=y_right).start()
        fill_ring(n, 0, 1, y_far)
        r_copy(n, to_ring.at[n, 0, 1], far_in.at[n, 1], 1, y=y_left).start()

    def sums_left(n):
        core_copy(n, y_left, 1).wait_recv()
        fill_ring(n, 1, 0, y_left)
        r_copy(n, to_ring.at[n, 1, 0], near_in.at[n, 1, 0], 2, y=y_left).start()

    def sums_right(n):
        core_copy(n, y_right, 2).wait_recv()
        fill_ring(n, 2, 1, y_right)
        r_copy(n, to_ring.at[n, 2, 1], near_in.at[n, 0, 1], 3, y=y_right).start()

    def sums_near(n):
        r_copy(n, far_in.at[n, 0], far_in.at[n, 0], 0, y=y_right).wait_recv()
        fill_ring(n, 2, 0, y_right, far_in.at[n, 0])
        r_copy(n, to_ring.at[n, 2, 0], near_in.at[n, 0, 0], 4, y=y_right).start()
        r_copy(n, far_in.at[n, 1], far_in.at[n, 1], 1, y=y_right).wait_recv()
        fill_ring(n, 1, 1, y_left, far_in.at[n, 1])
        r_copy(n, to_ring.at[n, 1, 1], near_in.at[n, 1, 1], 5, y=y_left).start()

    def near_wait(n, side, q):
        k = ((4, 3), (2, 5))[side][q]
        ref = near_in.at[n, side, q]
        r_copy(n, ref, ref, k, y=y_right).wait_recv()

    def sums_sent(n):
        for k in range(4):
            core_copy(n, y, k).wait_send()
        for k in range(6):
            r_copy(n, to_ring.at[n, 0, 0], to_ring.at[n, 0, 0], k, y=y_right).wait_send()

    def sums_wait(n):
        core_copy(n, y, 3).wait_recv()
        for side in (0, 1):
            for q in (0, 1):
                near_wait(n, side, q)

    def own_sum(n, q, at_row):
        total = chip_sum(n, y, q * QUARTER + at_row)
        for side in (0, 1):
            total = total + near_in[n, side, q, at_row : at_row + 16, :].astype(F32)
        return total

    def first_norm(h):
        for q in (0, 1):
            for at_row in range(0, QUARTER, 16):
                here = h * HALF + q * QUARTER + at_row
                wide = resid[here : here + 16, :].astype(F32)
                rows_g[h, y, c, q, at_row : at_row + 16, :] = rms_rows(wide, mix_gain[...])

    def gate_map():
        gate_w[...] = jnp.zeros_like(gate_w)
        for n in range(recur_w.shape[0]):
            block = slice(n * GATE_BLOCK, (n + 1) * GATE_BLOCK)
            gate_w[block, block] = recur_w[n]
            block_two = slice(256 + n * GATE_BLOCK, 256 + (n + 1) * GATE_BLOCK)
            gate_w[block, block_two] = input_w[n]

    def turn_up():
        own_copy(5).wait()
        own_copy(6).wait()
        for b in range(11):
            if b < 5:
                tile = gate_in[b * 128 : (b + 1) * 128, :]
            elif b < 10:
                tile = value_in[(b - 5) * 128 : (b - 4) * 128, :]
            else:
                tile = jnp.concatenate([gate_in[640:704, :], value_in[640:704, :]], axis=0)
            up_g[z, x, :, b * 128 : (b + 1) * 128] = tile.astype(F32).T.astype(BF16)

    def recur(h, g):
        w = in_g[...].reshape(-1, 256)
        proj[...] = jnp.dot(group_rows(h, g), w, preferred_element_type=F32)
        taps = conv_taps[...]
        blocks = [(j, s) for j in range(2) for s in range(2)]
        for j, s in blocks:
            yq = group(g)[j]
            rows = slice((2 * j + s) * HALF, (2 * j + s + 1) * HALF)
            wide = proj[rows, :].astype(BF16).astype(F32)
            before = jnp.zeros((8, 256), F32) if h == 0 else conv_tail[yq, s]
            if h == 0:
                conv_tail[yq, s] = wide[HALF - 8 :]
            extended = jnp.concatenate([before, wide], axis=0)
            conv = behind(extended, 3) * taps[0:1]
            conv = conv + behind(extended, 2) * taps[1:2]
            conv = conv + behind(extended, 1) * taps[2:3]
            proj[rows, :] = conv + wide * taps[3:4]
        gates[...] = jnp.dot(proj[...].astype(BF16), gate_w[...], preferred_element_type=F32)
        for j, s in blocks:
            yq = group(g)[j]
            rows = slice((2 * j + s) * HALF, (2 * j + s + 1) * HALF)
            for b in range(2):
                lanes = slice(b * 128, (b + 1) * 128)
                lanes2 = slice(256 + b * 128, 256 + (b + 1) * 128)
                rgate = jax.nn.sigmoid(gates[rows, lanes])
                igate = jax.nn.sigmoid(gates[rows, lanes2])
                a = 8.0 * rgate * decay_rate[:, lanes]
                decay = jnp.exp(-a)
                a2 = a * a
                series = 1.0 + a2 * (1.0 / 6) * (1.0 + a2 * (1.0 / 20) * (1.0 + a2 * (1.0 / 42)))
                left_over = jnp.where(a < 0.3, 2.0 * decay * (a * series), 1.0 - decay * decay)
                state = jnp.sqrt(left_over) * (igate * proj[rows, lanes])
                pos = lax.broadcasted_iota(jnp.int32, state.shape, 0)
                if h == 1:
                    state = state + jnp.where(pos == 0, decay * carry[yq, s, 0:1, lanes], 0.0)
                by = 1
                while by < HALF:
                    state = decay * shifted(state, pos, by, 0.0) + state
                    if 2 * by < HALF:
                        decay = decay * shifted(decay, pos, by, 1.0)
                    by *= 2
                if h == 0:
                    carry[yq, s, 0:1, lanes] = state[HALF - 1 :]
                recurred[h, yq, s * HALF : (s + 1) * HALF, lanes] = state.astype(BF16)

    def product(n, g, left, table, order):
        rows = jnp.concatenate([left[n % 2, yq] for yq in group(g)], axis=0)
        for zq in range(RING):
            w = jnp.concatenate([table[zq, xq] for xq in range(RING)], axis=1)
            term = jnp.dot(rows, w, preferred_element_type=F32).astype(BF16)
            for j, yq in enumerate(group(g)):
                for s in range(2):
                    lo = (2 * j + s) * HALF
                    partial[n, yq, s, :, zq * 512 : (zq + 1) * 512] = term[lo : lo + HALF]
        for j, k in order:
            core_copy(n, group(g)[j], k).start()

    def products(n, left, table):
        product(n, 1, left, table, ((1, 0), (0, 1)))
        sums_far(n)
        product(n, 0, left, table, ((1, 2), (0, 3)))
        sums_left(n)
        sums_right(n)

    def mixed(h):
        products(h, recurred, out_g)

    def lowered(h):
        products(2 + h, hidden, down_g)

    def second_norm(h):
        sums_wait(h)
        for q in (0, 1):
            for at_row in range(0, QUARTER, 16):
                lo = h * HALF + q * QUARTER + at_row
                here = slice(lo, lo + 16)
                mid = (resid[here, :].astype(F32) + own_sum(h, q, at_row)).astype(BF16)
                middle[here, :] = mid
                out = rms_rows(mid.astype(F32), mlp_gain[...])
                rows_g[2 + h, y, c, q, at_row : at_row + 16, :] = out
        rows_send(2 + h)

    def gated(extended, value, taps):
        conv = behind(extended, 2) * taps[0:1]
        conv = conv + behind(extended, 1) * taps[1:2]
        conv = conv + extended[8:] * taps[2:3]
        return (conv / (1.0 + jnp.exp(-conv)) * value).astype(BF16)

    def feed(h, g):
        w = up_g[...].reshape(-1, 1408)
        pre[...] = jnp.dot(group_rows(2 + h, g), w, preferred_element_type=F32)
        for j in range(2):
            yq = group(g)[j]
            for s in range(2):
                rows = slice((2 * j + s) * HALF, (2 * j + s + 1) * HALF)
                out = slice(s * HALF, (s + 1) * HALF)
                for b in range(6):
                    lanes = slice(b * 128, (b + 1) * 128)
                    if b < 5:
                        gate = pre[rows, lanes].astype(BF16).astype(F32)
                        value = pre[rows, 640 + b * 128 : 640 + (b + 1) * 128]
                        value = value.astype(BF16).astype(F32)
                        taps = ffn_taps[:, lanes]
                    else:
                        gate = pre[rows, 1280:1408].astype(BF16).astype(F32)
                        value = pltpu.roll(gate, 64, axis=1)
                        taps = jnp.concatenate([ffn_taps[:, 640:704], jnp.zeros((3, 64), F32)], axis=1)
                    before = jnp.zeros((8, 128), F32) if h == 0 else gate_tail[yq, s, :, lanes]
                    if h == 0:
                        gate_tail[yq, s, :, lanes] = gate[HALF - 8 :]
                    unit = gated(jnp.concatenate([before, gate], axis=0), value, taps)
                    if b < 5:
                        hidden[h, yq, out, lanes] = unit
                    else:
                        hidden[h, yq, out, 640:704] = unit[:, :64]

    def finish(h):
        sums_wait(2 + h)
        for q in (0, 1):
            for at_row in range(0, QUARTER, 16):
                lo = h * HALF + q * QUARTER + at_row
                here = slice(lo, lo + 16)
                total = middle[here, :].astype(F32) + own_sum(2 + h, q, at_row)
                result[here, :] = total.astype(BF16)

    first_send(0)
    first_send(1)
    own_copy(4).wait()
    first_norm(0)
    rows_send(0)
    turn_up()
    first_send(2)
    gate_map()
    first_norm(1)
    first_forward(0)
    first_forward(1)
    rows_first(0)
    rows_send(1)
    second_send(0)
    second_send(1)
    first_send(3)
    rows_second(0)
    first_forward(2)
    second_forward(0)
    second_forward(1)
    rows_third(0)
    second_send(2)
    weights_done(0)
    recur(0, 0)
    recur(0, 1)
    rows_first(1)
    weights_done(1)
    mixed(0)
    rows_second(1)
    first_forward(3)
    rows_third(1)
    recur(1, 0)
    recur(1, 1)
    sums_near(0)
    mixed(1)
    second_send(3)
    second_norm(0)
    sums_near(1)
    second_forward(2)
    rows_first(2)
    rows_second(2)
    second_norm(1)
    rows_third(2)
    weights_done(2)
    feed(0, 0)
    feed(0, 1)
    rows_first(3)
    second_forward(3)
    rows_second(3)
    weights_done(3)
    lowered(0)
    rows_third(3)
    feed(1, 0)
    feed(1, 1)
    sums_near(2)
    lowered(1)
    finish(0)
    sums_near(3)
    finish(1)

    for n in range(4):
        rows_sent(n)
        sums_sent(n)
    for i in range(4):
        weights_sent(i)


def shards(
    resid,
    mix_gain,
    in_weight,
    conv_taps,
    recur_gate_w,
    input_gate_w,
    decay_rate,
    out_weight,
    mlp_gain,
    up_gate_w,
    up_val_w,
    ffn_taps,
    down_weight,
):
    vmem = pl.BlockSpec(memory_space=pltpu.VMEM)
    hbm = pl.BlockSpec(memory_space=pl.ANY)
    dma = pltpu.SemaphoreType.DMA
    width = resid.shape[1]
    units = up_gate_w.shape[1]
    return pl.pallas_call(
        kernel,
        name="layer",
        out_shape=jax.ShapeDtypeStruct(resid.shape, BF16),
        in_specs=[hbm, vmem, hbm, vmem, vmem, vmem, vmem, hbm, vmem, hbm, hbm, vmem, hbm],
        out_specs=vmem,
        scratch_shapes=[
            pltpu.VMEM(resid.shape, BF16),
            pltpu.VMEM((units, 128), BF16),
            pltpu.VMEM((units, 128), BF16),
            pltpu.VMEM((RING, RING, *in_weight.shape), BF16),
            pltpu.VMEM((RING, RING, *out_weight.shape), BF16),
            pltpu.VMEM((RING, RING, up_gate_w.shape[0], 2 * units), BF16),
            pltpu.VMEM((RING, RING, *down_weight.shape), BF16),
            pltpu.VMEM((4, RING, 2, 2, QUARTER, width), BF16),
            pltpu.VMEM((256, 512), BF16),
            pltpu.VMEM((4 * HALF, 256), F32),
            pltpu.VMEM((4 * HALF, 512), F32),
            pltpu.VMEM((RING, 2, 8, 256), F32),
            pltpu.VMEM((RING, 2, 8, 256), F32),
            pltpu.VMEM((2, RING, 2 * HALF, 256), BF16),
            pltpu.VMEM((4 * HALF, 2 * units), F32),
            pltpu.VMEM((RING, 2, 8, 768), F32),
            pltpu.VMEM((2, RING, 2 * HALF, units), BF16),
            pltpu.VMEM((4, RING, 2, HALF, width), BF16),
            pltpu.VMEM((4, RING, HALF, width), BF16),
            pltpu.VMEM((4, 3, 2, QUARTER, width), BF16),
            pltpu.VMEM((4, 2, QUARTER, width), BF16),
            pltpu.VMEM((4, 2, 2, QUARTER, width), BF16),
            pltpu.VMEM((SEQ, width), BF16),
            dma((4, 4, 6)),
            dma((4, 4, 6)),
            dma((7,)),
            dma((4, 14)),
            dma((4, 14)),
            dma((4, 4)),
            dma((4, 4)),
            dma((4, 6)),
            dma((4, 6)),
        ],
        compiler_params=pltpu.CompilerParams(
            collective_id=0, has_side_effects=True, vmem_limit_bytes=60 * 1024 * 1024
        ),
    )(
        resid,
        mix_gain[None],
        in_weight,
        conv_taps,
        recur_gate_w,
        input_gate_w,
        decay_rate[None],
        out_weight,
        mlp_gain[None],
        up_gate_w.T,
        up_val_w.T,
        ffn_taps,
        down_weight,
    )


def solution(mesh):
    split = Mesh(mesh.devices.reshape(RING, RING, RING, 2), ("z", "x", "y", "c"))
    fs, tp = ("z", "x"), ("y", "c")
    rows = ("z", "x", "y", "c")
    return jax.shard_map(
        shards,
        mesh=split,
        in_specs=(
            P(rows, None),
            P(),
            P(fs, tp),
            P(None, tp),
            P(tp, None, None),
            P(tp, None, None),
            P(tp),
            P(tp, fs),
            P(),
            P(fs, tp),
            P(fs, tp),
            P(None, tp),
            P(tp, fs),
        ),
        out_specs=P(rows, None),
        check_vma=False,
    )
```

time: 118 us -> 103 us (0.87)
  Pallas kernels: 110 us -> 101 us
  local copies, waits for them, and re-layouts: 7.83 us -> 1.88 us
    pallas_call x1, Pallas kernels: 110 us -> 101 us  [shards(): pl.pallas_call(kernel, name='layer', out_shape=jax.ShapeDtypeStruct(resid...]
    slice x8 -> x0, local copies, waits for them, and re-layouts: 3.27 us -> none  [the longest x2 0.92 us: shards(): up_gate_w[:, :640]]
    pad x1 -> x0, local copies, waits for them, and re-layouts: 1.3 us -> none  [shards(): taps = jnp.pad(ffn_taps, ((0, 0), (0, 64)))]
    unnamed x5 -> x1, local copies, waits for them, and re-layouts: 2.43 us -> 1.88 us
where the time goes in v2:
time: 103 us
  Pallas kernels  101 us (98%)
  local copies, waits for them, and re-layouts  1.88 us (2%)
    pallas_call x1, Pallas kernels, shards(): pl.pallas_call(kernel, name='layer', out_shape=jax.ShapeDtypeStruct(resid...  101 us

profile of v2, /device:TPU:1, one launch (start us, length us, event | category | flops | bytes accessed | tf_op | source)
XLA Modules:
  0.0 102.8 jit_solution(8933049846560504659)
XLA Ops:
  0.0 100.9 %layer.1 = bf16[128,2048]{1,0:T(8,128)(2,1)} custom-call(bf16[128,2048]{1,0:T(8,128)(2,1)} %resid_hbm.1, f32[1,2048]{1,0:T(1,128)} %bitcast.7, bf16[128,256]{1,0:T(8,128)(2,1)} %in_w.1, f32[4,256]{1,0:T(4,128)} %conv_taps.1, bf16[4,64,64]{2,1,0:T(8,128)(2,1)} %recur_w.1, bf16[4,64,64]{2,1,0:T(8,128)(2,1)} %input_w.1, f32[1,256]{1,0:T(1,128)} %bitcast.9, ...), custom_call_target="tpu_custom_call" | custom-call | tf_op jit(solution)/shard_map/layer/pallas_call | solution.py:556
  100.9 1.9 %copy.15 = bf16[128,2048]{1,0:T(8,128)(2,1)} copy(bf16[128,2048]{1,0:T(8,128)(2,1)} %layer.1) | data formatting | bytes 1048576

commit v3 on v2

--- a/solution.py
+++ b/solution.py
@@ -16,6 +16,120 @@
 F32 = jnp.float32
 
 OWN, RIGHT, LEFT, FAR, IN_RIGHT, IN_LEFT, IN_FAR = 0, 2, 4, 6, 8, 10, 12
+
+
+ORDER = (
+    ("S1", 0),
+    ("RS", 1),
+    ("RS", 0),
+    ("S1", 1),
+    ("S1", 3),
+    ("F1", 0, 3),
+    ("F1", 0, 0),
+    ("F1", 1, 0),
+    ("F1", 1, 2),
+    ("S1", 2),
+    ("F1", 0, 1),
+    ("F1", 1, 1),
+    ("S2", 0, 3),
+    ("F1", 1, 3),
+    ("F1", 0, 2),
+    ("S2", 1, 0),
+    ("S2", 0, 0),
+    ("S2", 1, 2),
+    ("S2", 0, 2),
+    ("F1", 3, 3),
+    ("F1", 3, 1),
+    ("F1", 2, 0),
+    ("F1", 2, 2),
+    ("S2", 0, 1),
+    ("S2", 1, 1),
+    ("F1", 2, 3),
+    ("R1", 0),
+    ("R2", 1),
+    ("S2", 1, 3),
+    ("R2", 0),
+    ("F2", 0, 0),
+    ("F2", 1, 0),
+    ("F2", 0, 3),
+    ("F2", 0, 1),
+    ("F2", 0, 2),
+    ("F2", 1, 2),
+    ("R1", 1),
+    ("F1", 2, 1),
+    ("F2", 1, 3),
+    ("S2", 3, 3),
+    ("F1", 3, 0),
+    ("F2", 1, 1),
+    ("S2", 2, 0),
+    ("R3", 0),
+    ("S2", 2, 1),
+    ("F1", 3, 2),
+    ("D", 0),
+    ("rec", 0, 1),
+    ("S2", 2, 3),
+    ("D", 1),
+    ("S2", 2, 2),
+    ("R3", 1),
+    ("prod", 0, 1),
+    ("rec", 0, 0),
+    ("prod", 0, 0),
+    ("sfar", 0),
+    ("S2", 3, 1),
+    ("rec", 1, 1),
+    ("sright", 0),
+    ("sleft", 0),
+    ("prod", 1, 1),
+    ("rec", 1, 0),
+    ("near", 0),
+    ("prod", 1, 0),
+    ("sfar", 1),
+    ("sleft", 1),
+    ("sright", 1),
+    ("F2", 2, 1),
+    ("S2", 3, 0),
+    ("F2", 2, 3),
+    ("F2", 2, 0),
+    ("S2", 3, 2),
+    ("norm2", 0),
+    ("near", 1),
+    ("F2", 2, 2),
+    ("RS", 2),
+    ("R1", 2),
+    ("F2", 3, 2),
+    ("F2", 3, 0),
+    ("norm2", 1),
+    ("F2", 3, 3),
+    ("F2", 3, 1),
+    ("R2", 2),
+    ("RS", 3),
+    ("R3", 2),
+    ("D", 2),
+    ("feed", 0, 0),
+    ("R1", 3),
+    ("feed", 0, 1),
+    ("D", 3),
+    ("prod", 2, 1),
+    ("prod", 2, 0),
+    ("sfar", 2),
+    ("R3", 3),
+    ("R2", 3),
+    ("sleft", 2),
+    ("sright", 2),
+    ("feed", 1, 1),
+    ("prod", 3, 1),
+    ("near", 2),
+    ("feed", 1, 0),
+    ("sfar", 3),
+    ("prod", 3, 0),
+    ("sright", 3),
+    ("sleft", 3),
+    ("sent",),
+    ("near", 3),
+    ("fin", 0),
+    ("fin", 1),
+)
+WAITED = {0: 3, 1: 0, 3: 3}
 
 
 def remote(src, dst, send_sem, recv_sem, **device):
@@ -44,22 +158,30 @@
 
 def kernel(
     resid_hbm,
+    mix_gain_hbm,
+    in_w,
+    conv_taps_hbm,
+    recur_w_hbm,
+    input_w_hbm,
+    decay_rate_hbm,
+    out_w,
+    mlp_gain_hbm,
+    gate_t,
+    value_t,
+    ffn_taps_hbm,
+    down_w,
+    result_hbm,
+    resid,
+    gate_in,
+    value_in,
     mix_gain,
-    in_w,
     conv_taps,
     recur_w,
     input_w,
     decay_rate,
-    out_w,
     mlp_gain,
-    gate_t,
-    value_t,
     ffn_taps,
-    down_w,
     result,
-    resid,
-    gate_in,
-    value_in,
     in_g,
     out_g,
     up_g,
@@ -105,10 +227,25 @@
         if i < 4:
             src, g = weights[i]
             return pltpu.make_async_copy(src, g.at[z, x], l_sem.at[i])
-        src, dst = ((resid_hbm, resid), (gate_t, gate_in), (value_t, value_in))[i - 4]
+        src, dst = (
+            (resid_hbm, resid),
+            (gate_t, gate_in),
+            (value_t, value_in),
+            (mix_gain_hbm, mix_gain),
+            (recur_w_hbm, recur_w),
+            (input_w_hbm, input_w),
+            (conv_taps_hbm, conv_taps),
+            (decay_rate_hbm, decay_rate),
+            (mlp_gain_hbm, mlp_gain),
+            (ffn_taps_hbm, ffn_taps),
+        )[i - 4]
         return pltpu.make_async_copy(src, dst, l_sem.at[i])
 
-    for i in (4, 5, 6, 0, 1, 3):
+    def result_copy(h):
+        here = pl.ds(h * HALF, HALF)
+        return pltpu.make_async_copy(result.at[here], result_hbm.at[here], l_sem.at[14 + h])
+
+    for i in (4, 7, 5, 6, 8, 9, 10, 11, 12, 13, 0, 1, 3):
         own_copy(i).start()
 
     barrier = pltpu.get_barrier_semaphore()
@@ -118,7 +255,6 @@
                 barrier, inc=1, device_id={axis: nxt(axis, by)}, device_id_type=MESH
             )
     pl.semaphore_signal(barrier, inc=1, device_id={"c": other}, device_id_type=MESH)
-    pl.semaphore_wait(barrier, 7)
 
     def piece(i, p):
         rows = weights[i][1].shape[2] // 4
@@ -155,39 +291,36 @@
         there = slot(i, p, axis, (-1, 1, 2)[k])
         w_copy(i, p, there, there, k, axis, 1).wait_recv()
 
-    def first_forward(i):
-        for p in range(4):
-            axis = axes_of(p)[0]
-            k = p % 2
-            first_wait(i, p, k)
-            by = 1 if k == 0 else -1
-            there = slot(i, p, axis, -by)
-            w_copy(i, p, there, there, 2, axis, by).start()
-
-    def second_send(i):
-        if weights[i][0] is not None:
+    def first_forward(i, p):
+        axis = axes_of(p)[0]
+        k = p % 2
+        first_wait(i, p, k)
+        by = 1 if k == 0 else -1
+        there = slot(i, p, axis, -by)
+        w_copy(i, p, there, there, 2, axis, by).start()
+
+    def second_send(i, p):
+        if p == WAITED.get(i):
             own_copy(i).wait()
-        for p in range(4):
-            axis = axes_of(p)[1]
-            first_wait(i, p, 1 - p % 2)
-            first_wait(i, p, 2)
-            here = line(i, p, axis, 0)
-            for k, by in ((3, 1), (4, -1)):
-                w_copy(i, p, here, here, k, axis, by).start()
+        axis = axes_of(p)[1]
+        first_wait(i, p, 1 - p % 2)
+        first_wait(i, p, 2)
+        here = line(i, p, axis, 0)
+        for k, by in ((3, 1), (4, -1)):
+            w_copy(i, p, here, here, k, axis, by).start()
 
     def second_wait(i, p, k):
         axis = axes_of(p)[1]
         there = line(i, p, axis, (-1, 1, 2)[k - 3])
         w_copy(i, p, there, there, k, axis, 1).wait_recv()
 
-    def second_forward(i):
-        for p in range(4):
-            axis = axes_of(p)[1]
-            k = 3 + p % 2
-            second_wait(i, p, k)
-            by = 1 if k == 3 else -1
-            there = line(i, p, axis, -by)
-            w_copy(i, p, there, there, 5, axis, by).start()
+    def second_forward(i, p):
+        axis = axes_of(p)[1]
+        k = 3 + p % 2
+        second_wait(i, p, k)
+        by = 1 if k == 3 else -1
+        there = line(i, p, axis, -by)
+        w_copy(i, p, there, there, 5, axis, by).start()
 
     def weights_done(i):
         for p in range(4):
@@ -330,8 +463,6 @@
             gate_w[block, block_two] = input_w[n]
 
     def turn_up():
-        own_copy(5).wait()
-        own_copy(6).wait()
         for b in range(11):
             if b < 5:
                 tile = gate_in[b * 128 : (b + 1) * 128, :]
@@ -398,18 +529,12 @@
         for j, k in order:
             core_copy(n, group(g)[j], k).start()
 
-    def products(n, left, table):
-        product(n, 1, left, table, ((1, 0), (0, 1)))
-        sums_far(n)
-        product(n, 0, left, table, ((1, 2), (0, 3)))
-        sums_left(n)
-        sums_right(n)
-
-    def mixed(h):
-        products(h, recurred, out_g)
-
-    def lowered(h):
-        products(2 + h, hidden, down_g)
+    def step_product(n, g):
+        order = ((1, 2), (0, 3)) if g == 0 else ((1, 0), (0, 1))
+        if n < 2:
+            product(n, g, recurred, out_g, order)
+        else:
+            product(n, g, hidden, down_g, order)
 
     def second_norm(h):
         sums_wait(h)
@@ -421,7 +546,6 @@
                 middle[here, :] = mid
                 out = rms_rows(mid.astype(F32), mlp_gain[...])
                 rows_g[2 + h, y, c, q, at_row : at_row + 16, :] = out
-        rows_send(2 + h)
 
     def gated(extended, value, taps):
         conv = behind(extended, 2) * taps[0:1]
@@ -465,72 +589,56 @@
                 here = slice(lo, lo + 16)
                 total = middle[here, :].astype(F32) + own_sum(2 + h, q, at_row)
                 result[here, :] = total.astype(BF16)
-
-    first_send(0)
-    first_send(1)
+        result_copy(h).start()
+
     own_copy(4).wait()
+    own_copy(7).wait()
     first_norm(0)
-    rows_send(0)
+    own_copy(5).wait()
+    own_copy(6).wait()
     turn_up()
-    first_send(2)
+    own_copy(8).wait()
+    own_copy(9).wait()
     gate_map()
     first_norm(1)
-    first_forward(0)
-    first_forward(1)
-    rows_first(0)
-    rows_send(1)
-    second_send(0)
-    second_send(1)
-    first_send(3)
-    rows_second(0)
-    first_forward(2)
-    second_forward(0)
-    second_forward(1)
-    rows_third(0)
-    second_send(2)
-    weights_done(0)
-    recur(0, 0)
-    recur(0, 1)
-    rows_first(1)
-    weights_done(1)
-    mixed(0)
-    rows_second(1)
-    first_forward(3)
-    rows_third(1)
-    recur(1, 0)
-    recur(1, 1)
-    sums_near(0)
-    mixed(1)
-    second_send(3)
-    second_norm(0)
-    sums_near(1)
-    second_forward(2)
-    rows_first(2)
-    rows_second(2)
-    second_norm(1)
-    rows_third(2)
-    weights_done(2)
-    feed(0, 0)
-    feed(0, 1)
-    rows_first(3)
-    second_forward(3)
-    rows_second(3)
-    weights_done(3)
-    lowered(0)
-    rows_third(3)
-    feed(1, 0)
-    feed(1, 1)
-    sums_near(2)
-    lowered(1)
-    finish(0)
-    sums_near(3)
-    finish(1)
-
-    for n in range(4):
-        rows_sent(n)
-        sums_sent(n)
-    for i in range(4):
-        weights_sent(i)
+    for i in (10, 11, 12, 13):
+        own_copy(i).wait()
+    pl.semaphore_wait(barrier, 7)
+
+    def sent():
+        for n in range(4):
+            rows_sent(n)
+            if n < 3:
+                sums_sent(n)
+        for i in range(4):
+            weights_sent(i)
+
+    steps = {
+        "S1": first_send,
+        "F1": first_forward,
+        "S2": second_send,
+        "F2": second_forward,
+        "D": weights_done,
+        "RS": rows_send,
+        "R1": rows_first,
+        "R2": rows_second,
+        "R3": rows_third,
+        "rec": recur,
+        "feed": feed,
+        "prod": step_product,
+        "sfar": sums_far,
+        "sleft": sums_left,
+        "sright": sums_right,
+        "near": sums_near,
+        "norm2": second_norm,
+        "fin": finish,
+        "sent": sent,
+    }
+    for name, *where in ORDER:
+        steps[name](*where)
+    sums_sent(3)
+    result_copy(0).wait()
+    result_copy(1).wait()
 
 
 def shards(
@@ -548,7 +656,6 @@
     ffn_taps,
     down_weight,
 ):
-    vmem = pl.BlockSpec(memory_space=pltpu.VMEM)
     hbm = pl.BlockSpec(memory_space=pl.ANY)
     dma = pltpu.SemaphoreType.DMA
     width = resid.shape[1]
@@ -556,13 +663,21 @@
     return pl.pallas_call(
         kernel,
         name="layer",
-        out_shape=jax.ShapeDtypeStruct(resid.shape, BF16),
-        in_specs=[hbm, vmem, hbm, vmem, vmem, vmem, vmem, hbm, vmem, hbm, hbm, vmem, hbm],
-        out_specs=vmem,
+        out_shape=pltpu.VMEM(resid.shape, BF16),
+        in_specs=[hbm] * 13,
+        out_specs=pl.BlockSpec(memory_space=pltpu.VMEM),
         scratch_shapes=[
             pltpu.VMEM(resid.shape, BF16),
             pltpu.VMEM((units, 128), BF16),
             pltpu.VMEM((units, 128), BF16),
+            pltpu.VMEM((1, width), F32),
+            pltpu.VMEM(conv_taps.shape, F32),
+            pltpu.VMEM(recur_gate_w.shape, BF16),
+            pltpu.VMEM(input_gate_w.shape, BF16),
+            pltpu.VMEM((1, *decay_rate.shape), F32),
+            pltpu.VMEM((1, width), F32),
+            pltpu.VMEM(ffn_taps.shape, F32),
+            pltpu.VMEM(resid.shape, BF16),
             pltpu.VMEM((RING, RING, *in_weight.shape), BF16),
             pltpu.VMEM((RING, RING, *out_weight.shape), BF16),
             pltpu.VMEM((RING, RING, up_gate_w.shape[0], 2 * units), BF16),
@@ -585,7 +700,7 @@
             pltpu.VMEM((SEQ, width), BF16),
             dma((4, 4, 6)),
             dma((4, 4, 6)),
-            dma((7,)),
+            dma((16,)),
             dma((4, 14)),
             dma((4, 14)),
             dma((4, 4)),
@@ -594,7 +709,7 @@
             dma((4, 6)),
         ],
         compiler_params=pltpu.CompilerParams(
-            collective_id=0, has_side_effects=True, vmem_limit_bytes=60 * 1024 * 1024
+            collective_id=0, has_side_effects=True, vmem_limit_bytes=56 * 1024 * 1024
         ),
     )(
         resid,

time: 103 us -> 93.5 us (0.908)
  Pallas kernels: 101 us -> 92.6 us
  local copies, waits for them, and re-layouts: 1.88 us -> 0.8 us
    pallas_call x1, Pallas kernels: 101 us -> 92.6 us  [shards(): pl.pallas_call(kernel, name='layer', out_shape=pltpu.VMEM(resid.shape, BF...]
    unnamed x1, local copies, waits for them, and re-layouts: 1.88 us -> 0.8 us
where the time goes in v3:
time: 93.5 us; the launch traced here: 93.4 us
  Pallas kernels  92.6 us (99%)
    pallas_call x1, Pallas kernels, shards(): pl.pallas_call(kernel, name='layer', out_shape=pltpu.VMEM(resid.shape, BF...  92.6 us

profile of v3, /device:TPU:1, one launch (start us, length us, event | category | flops | bytes accessed | tf_op | source)
XLA Modules:
  0.0 93.4 jit_solution(6123820489795109234)
XLA Ops:
  0.0 92.6 %layer.1 = bf16[128,2048]{1,0:T(8,128)(2,1)S(1)} custom-call(bf16[128,2048]{1,0:T(8,128)(2,1)} %resid_hbm.1, f32[1,2048]{1,0:T(1,128)} %bitcast.7, bf16[128,256]{1,0:T(8,128)(2,1)} %in_w.1, f32[4,256]{1,0:T(4,128)} %conv_taps_hbm.1, bf16[4,64,64]{2,1,0:T(8,128)(2,1)} %recur_w_hbm.1, bf16[4,64,64]{2,1,0:T(8,128)(2,1)} %input_w_hbm.1, f32[1,256]{1,0:T(1,128)} %bitcast.9, ...), custom_call_target="tpu_custom_call" | custom-call | tf_op jit(solution)/shard_map/layer/pallas_call | solution.py:663
  92.6 0.8 copy.15

commit v4 on v3

--- a/solution.py
+++ b/solution.py
@@ -18,118 +18,154 @@
 OWN, RIGHT, LEFT, FAR, IN_RIGHT, IN_LEFT, IN_FAR = 0, 2, 4, 6, 8, 10, 12
 
 
+PIECES = (4, 4, 4, 4)
+X_FIRST = (2, 2, 2, 2)
+SUMS = ((0, 0, 16), (1, 0, 16), (2, 0, 9), (3, 0, 9), (2, 9, 16), (3, 9, 16))
+BLOCKS = tuple(
+    sorted(((dz, dx) for dz in (0, 1, -1, 2) for dx in (0, 1, -1, 2)), key=lambda d: 2 in d)
+)
 ORDER = (
-    ("S1", 0),
-    ("RS", 1),
+    ("S1", 0, 1),
+    ("S1", 1, 0),
+    ("S1", 1, 3),
     ("RS", 0),
-    ("S1", 1),
-    ("S1", 3),
+    ("S1", 0, 3),
+    ("S1", 0, 0),
+    ("S1", 1, 2),
+    ("S1", 0, 2),
+    ("S1", 1, 1),
+    ("S1", 2, 2),
+    ("S1", 2, 0),
+    ("F1", 1, 3),
+    ("F1", 1, 0),
     ("F1", 0, 3),
     ("F1", 0, 0),
-    ("F1", 1, 0),
+    ("S1", 2, 3),
+    ("RS", 1),
+    ("S1", 2, 1),
+    ("S1", 3, 1),
     ("F1", 1, 2),
-    ("S1", 2),
+    ("F1", 0, 2),
     ("F1", 0, 1),
+    ("F1", 2, 2),
+    ("F1", 2, 0),
+    ("S2", 0, 3),
     ("F1", 1, 1),
-    ("S2", 0, 3),
-    ("F1", 1, 3),
-    ("F1", 0, 2),
     ("S2", 1, 0),
     ("S2", 0, 0),
+    ("S2", 0, 1),
+    ("S2", 0, 2),
+    ("S2", 1, 3),
     ("S2", 1, 2),
-    ("S2", 0, 2),
-    ("F1", 3, 3),
+    ("S2", 1, 1),
+    ("R1", 0),
+    ("F1", 2, 3),
     ("F1", 3, 1),
-    ("F1", 2, 0),
-    ("F1", 2, 2),
-    ("S2", 0, 1),
-    ("S2", 1, 1),
-    ("F1", 2, 3),
-    ("R1", 0),
+    ("F2", 0, 3),
     ("R2", 1),
-    ("S2", 1, 3),
+    ("F2", 0, 0),
+    ("F2", 0, 2),
+    ("F2", 0, 1),
+    ("F2", 1, 1),
+    ("R1", 1),
+    ("F2", 1, 3),
+    ("F2", 1, 0),
+    ("R3", 0),
+    ("F2", 1, 2),
+    ("F1", 2, 1),
+    ("S1", 3, 2),
     ("R2", 0),
-    ("F2", 0, 0),
-    ("F2", 1, 0),
-    ("F2", 0, 3),
-    ("F2", 0, 1),
-    ("F2", 0, 2),
-    ("F2", 1, 2),
-    ("R1", 1),
-    ("F1", 2, 1),
-    ("F2", 1, 3),
-    ("S2", 3, 3),
-    ("F1", 3, 0),
-    ("F2", 1, 1),
+    ("S1", 3, 0),
+    ("S1", 3, 3),
     ("S2", 2, 0),
-    ("R3", 0),
-    ("S2", 2, 1),
-    ("F1", 3, 2),
-    ("D", 0),
+    ("S2", 2, 2),
+    ("DA", 1),
+    ("DA", 0),
+    ("DB", 0),
     ("rec", 0, 1),
-    ("S2", 2, 3),
-    ("D", 1),
-    ("S2", 2, 2),
     ("R3", 1),
+    ("DB", 1),
     ("prod", 0, 1),
     ("rec", 0, 0),
+    ("sfar", 0),
     ("prod", 0, 0),
-    ("sfar", 0),
+    ("S2", 2, 3),
+    ("sleft", 0),
+    ("F1", 3, 3),
+    ("F1", 3, 2),
+    ("sright", 0),
+    ("rec", 1, 1),
+    ("S2", 2, 1),
+    ("prod", 1, 1),
+    ("near", 0),
+    ("sfar", 1),
+    ("S2", 3, 2),
+    ("F2", 2, 0),
+    ("F1", 3, 0),
     ("S2", 3, 1),
-    ("rec", 1, 1),
-    ("sright", 0),
-    ("sleft", 0),
-    ("prod", 1, 1),
     ("rec", 1, 0),
-    ("near", 0),
+    ("sleft", 1),
+    ("F2", 2, 2),
     ("prod", 1, 0),
-    ("sfar", 1),
-    ("sleft", 1),
     ("sright", 1),
-    ("F2", 2, 1),
-    ("S2", 3, 0),
-    ("F2", 2, 3),
-    ("F2", 2, 0),
-    ("S2", 3, 2),
     ("norm2", 0),
     ("near", 1),
-    ("F2", 2, 2),
     ("RS", 2),
+    ("F2", 2, 3),
+    ("F2", 2, 1),
+    ("norm2", 1),
+    ("S2", 3, 3),
+    ("DA", 2),
     ("R1", 2),
+    ("S2", 3, 0),
+    ("F2", 3, 1),
+    ("RS", 3),
+    ("DB", 2),
+    ("R2", 2),
     ("F2", 3, 2),
-    ("F2", 3, 0),
-    ("norm2", 1),
-    ("F2", 3, 3),
-    ("F2", 3, 1),
-    ("R2", 2),
-    ("RS", 3),
     ("R3", 2),
-    ("D", 2),
     ("feed", 0, 0),
     ("R1", 3),
+    ("F2", 3, 3),
+    ("F2", 3, 0),
+    ("DA", 3),
     ("feed", 0, 1),
-    ("D", 3),
+    ("R2", 3),
     ("prod", 2, 1),
     ("prod", 2, 0),
     ("sfar", 2),
     ("R3", 3),
-    ("R2", 3),
+    ("sright", 2),
     ("sleft", 2),
-    ("sright", 2),
+    ("DB", 3),
+    ("prod", 4, 1),
     ("feed", 1, 1),
+    ("sfar", 4),
+    ("near", 2),
+    ("prod", 5, 1),
+    ("prod", 4, 0),
     ("prod", 3, 1),
-    ("near", 2),
+    ("sfar", 5),
+    ("sright", 4),
+    ("sleft", 4),
+    ("near", 4),
     ("feed", 1, 0),
     ("sfar", 3),
+    ("sleft", 5),
+    ("prod", 5, 0),
+    ("fin", 2),
+    ("sright", 5),
+    ("near", 5),
+    ("sleft", 3),
     ("prod", 3, 0),
     ("sright", 3),
-    ("sleft", 3),
+    ("fin", 4),
+    ("near", 3),
     ("sent",),
-    ("near", 3),
-    ("fin", 0),
-    ("fin", 1),
+    ("fin", 5),
+    ("fin", 3),
 )
-WAITED = {0: 3, 1: 0, 3: 3}
+WAITED = {0: 3, 1: 0, 3: 2}
 
 
 def remote(src, dst, send_sem, recv_sem, **device):
@@ -170,7 +206,7 @@
     value_t,
     ffn_taps_hbm,
     down_w,
-    result_hbm,
+    result,
     resid,
     gate_in,
     value_in,
@@ -181,7 +217,6 @@
     decay_rate,
     mlp_gain,
     ffn_taps,
-    result,
     in_g,
     out_g,
     up_g,
@@ -241,10 +276,6 @@
         )[i - 4]
         return pltpu.make_async_copy(src, dst, l_sem.at[i])
 
-    def result_copy(h):
-        here = pl.ds(h * HALF, HALF)
-        return pltpu.make_async_copy(result.at[here], result_hbm.at[here], l_sem.at[14 + h])
-
     for i in (4, 7, 5, 6, 8, 9, 10, 11, 12, 13, 0, 1, 3):
         own_copy(i).start()
 
@@ -257,11 +288,11 @@
     pl.semaphore_signal(barrier, inc=1, device_id={"c": other}, device_id_type=MESH)
 
     def piece(i, p):
-        rows = weights[i][1].shape[2] // 4
+        rows = weights[i][1].shape[2] // PIECES[i]
         return pl.ds(p * rows, rows)
 
-    def axes_of(p):
-        return ("x", "z") if p < 2 else ("z", "x")
+    def axes_of(i, p):
+        return ("x", "z") if p < X_FIRST[i] else ("z", "x")
 
     def slot(i, p, axis, by):
         g = weights[i][1]
@@ -276,23 +307,24 @@
         return g.at[:, nxt("x", by), piece(i, p)]
 
     def w_copy(i, p, src, dst, k, axis, by):
-        return remote(src, dst, w_send.at[i, p, k], w_recv.at[i, p, k], **{axis: nxt(axis, by)})
-
-    def first_send(i):
+        return remote(
+            src, dst, w_send.at[i, k // 3], w_recv.at[i, p, k], **{axis: nxt(axis, by)}
+        )
+
+    def first_send(i, p):
         src = weights[i][0]
-        for p in range(4):
-            axis = axes_of(p)[0]
-            here = slot(i, p, axis, 0)
-            for k, by in ((0, 1), (1, -1)):
-                w_copy(i, p, here if src is None else src.at[piece(i, p)], here, k, axis, by).start()
+        axis = axes_of(i, p)[0]
+        here = slot(i, p, axis, 0)
+        for k, by in ((0, 1), (1, -1)):
+            w_copy(i, p, here if src is None else src.at[piece(i, p)], here, k, axis, by).start()
 
     def first_wait(i, p, k):
-        axis = axes_of(p)[0]
+        axis = axes_of(i, p)[0]
         there = slot(i, p, axis, (-1, 1, 2)[k])
         w_copy(i, p, there, there, k, axis, 1).wait_recv()
 
     def first_forward(i, p):
-        axis = axes_of(p)[0]
+        axis = axes_of(i, p)[0]
         k = p % 2
         first_wait(i, p, k)
         by = 1 if k == 0 else -1
@@ -302,7 +334,7 @@
     def second_send(i, p):
         if p == WAITED.get(i):
             own_copy(i).wait()
-        axis = axes_of(p)[1]
+        axis = axes_of(i, p)[1]
         first_wait(i, p, 1 - p % 2)
         first_wait(i, p, 2)
         here = line(i, p, axis, 0)
@@ -310,34 +342,37 @@
             w_copy(i, p, here, here, k, axis, by).start()
 
     def second_wait(i, p, k):
-        axis = axes_of(p)[1]
+        axis = axes_of(i, p)[1]
         there = line(i, p, axis, (-1, 1, 2)[k - 3])
         w_copy(i, p, there, there, k, axis, 1).wait_recv()
 
     def second_forward(i, p):
-        axis = axes_of(p)[1]
+        axis = axes_of(i, p)[1]
         k = 3 + p % 2
         second_wait(i, p, k)
         by = 1 if k == 3 else -1
         there = line(i, p, axis, -by)
         w_copy(i, p, there, there, 5, axis, by).start()
 
-    def weights_done(i):
-        for p in range(4):
+    def weights_near(i):
+        for p in range(PIECES[i]):
             second_wait(i, p, 4 - p % 2)
+
+    def weights_far(i):
+        for p in range(PIECES[i]):
             second_wait(i, p, 5)
 
+    def all_sent(ref, sem):
+        pltpu.make_async_copy(ref, ref, sem).wait()
+
     def weights_sent(i):
-        for p in range(4):
-            first, second = axes_of(p)
-            one, four = slot(i, p, first, 0), line(i, p, second, 0)
-            for k in range(6):
-                ref = one if k < 3 else four
-                w_copy(i, p, ref, ref, k, first, 1).wait_send()
+        g = weights[i][1]
+        all_sent(g.at[0, pl.ds(0, 3)], w_send.at[i, 0])
+        all_sent(g.at[pl.ds(0, 3)], w_send.at[i, 1])
 
     def g_copy(n, yq, cq, q, s, r, **device):
         ref = rows_g.at[n, yq, cq, q]
-        return remote(ref, ref, g_send.at[n, s], g_recv.at[n, r], **device)
+        return remote(ref, ref, g_send.at[n, s // 12], g_recv.at[n, r], **device)
 
     def rows_wait(n, yq, cq, q, r):
         g_copy(n, yq, cq, q, 0, r, c=other).wait_recv()
@@ -368,8 +403,8 @@
             g_copy(n, y_far, c, q, 12 + q, FAR + q, c=other).start()
 
     def rows_sent(n):
-        for s in range(14):
-            g_copy(n, y, c, 0, s, 0, c=other).wait_send()
+        all_sent(rows_g.at[n, pl.ds(0, 3)], g_send.at[n, 0])
+        all_sent(rows_g.at[n, 3, 0], g_send.at[n, 1])
 
     def group(g):
         return (y, y_right) if g == 0 else (y_left, y_far)
@@ -380,71 +415,80 @@
                 rows_wait(n, yq, other, q, 4 * g + 2 * j + q)
         return jnp.concatenate([rows_g[n, yq].reshape(2 * HALF, -1) for yq in group(g)], axis=0)
 
-    def core_copy(n, yq, k):
+    def place(t):
+        n, lo, hi = SUMS[t]
+        return n, pl.ds(lo * 128, (hi - lo) * 128)
+
+    def core_copy(t, yq, k):
+        n, cols = place(t)
         return remote(
-            partial.at[n, yq, other], from_core.at[n, yq], c_send.at[n, k], c_recv.at[n, k], c=other
+            partial.at[n, yq, other, :, cols],
+            from_core.at[n, yq, :, cols],
+            c_send.at[t],
+            c_recv.at[t, k],
+            c=other,
         )
 
-    def r_copy(n, src, dst, k, **device):
-        return remote(src, dst, r_send.at[n, k], r_recv.at[n, k], **device)
-
-    def chip_sum(n, yq, at_row):
+    def ring_copy(t, j, q, k, side, **device):
+        n, cols = place(t)
+        there = far_in.at[n, q, :, cols] if side is None else near_in.at[n, side, q, :, cols]
+        return remote(to_ring.at[n, j, q, :, cols], there, r_send.at[t], r_recv.at[t, k], **device)
+
+    def chip_sum(t, yq, at_row):
+        n, cols = place(t)
         rows = pl.ds(at_row, 16)
-        return partial[n, yq, c, rows, :].astype(F32) + from_core[n, yq, rows, :].astype(F32)
-
-    def fill_ring(n, j, q, yq, extra=None):
+        return partial[n, yq, c, rows, cols].astype(F32) + from_core[n, yq, rows, cols].astype(F32)
+
+    def fill_ring(t, j, q, yq, far=False):
+        n, cols = place(t)
         for at_row in range(0, QUARTER, 16):
-            total = chip_sum(n, yq, q * QUARTER + at_row)
-            if extra is not None:
-                total = total + extra[at_row : at_row + 16, :].astype(F32)
-            to_ring[n, j, q, at_row : at_row + 16, :] = total.astype(BF16)
-
-    def sums_far(n):
-        core_copy(n, y_far, 0).wait_recv()
-        fill_ring(n, 0, 0, y_far)
-        r_copy(n, to_ring.at[n, 0, 0], far_in.at[n, 0], 0, y=y_right).start()
-        fill_ring(n, 0, 1, y_far)
-        r_copy(n, to_ring.at[n, 0, 1], far_in.at[n, 1], 1, y=y_left).start()
-
-    def sums_left(n):
-        core_copy(n, y_left, 1).wait_recv()
-        fill_ring(n, 1, 0, y_left)
-        r_copy(n, to_ring.at[n, 1, 0], near_in.at[n, 1, 0], 2, y=y_left).start()
-
-    def sums_right(n):
-        core_copy(n, y_right, 2).wait_recv()
-        fill_ring(n, 2, 1, y_right)
-        r_copy(n, to_ring.at[n, 2, 1], near_in.at[n, 0, 1], 3, y=y_right).start()
-
-    def sums_near(n):
-        r_copy(n, far_in.at[n, 0], far_in.at[n, 0], 0, y=y_right).wait_recv()
-        fill_ring(n, 2, 0, y_right, far_in.at[n, 0])
-        r_copy(n, to_ring.at[n, 2, 0], near_in.at[n, 0, 0], 4, y=y_right).start()
-        r_copy(n, far_in.at[n, 1], far_in.at[n, 1], 1, y=y_right).wait_recv()
-        fill_ring(n, 1, 1, y_left, far_in.at[n, 1])
-        r_copy(n, to_ring.at[n, 1, 1], near_in.at[n, 1, 1], 5, y=y_left).start()
-
-    def near_wait(n, side, q):
-        k = ((4, 3), (2, 5))[side][q]
-        ref = near_in.at[n, side, q]
-        r_copy(n, ref, ref, k, y=y_right).wait_recv()
-
-    def sums_sent(n):
-        for k in range(4):
-            core_copy(n, y, k).wait_send()
-        for k in range(6):
-            r_copy(n, to_ring.at[n, 0, 0], to_ring.at[n, 0, 0], k, y=y_right).wait_send()
-
-    def sums_wait(n):
-        core_copy(n, y, 3).wait_recv()
+            total = chip_sum(t, yq, q * QUARTER + at_row)
+            if far:
+                total = total + far_in[n, q, at_row : at_row + 16, cols].astype(F32)
+            to_ring[n, j, q, at_row : at_row + 16, cols] = total.astype(BF16)
+
+    def sums_far(t):
+        core_copy(t, y_far, 0).wait_recv()
+        fill_ring(t, 0, 0, y_far)
+        ring_copy(t, 0, 0, 0, None, y=y_right).start()
+        fill_ring(t, 0, 1, y_far)
+        ring_copy(t, 0, 1, 1, None, y=y_left).start()
+
+    def sums_left(t):
+        core_copy(t, y_left, 1).wait_recv()
+        fill_ring(t, 1, 0, y_left)
+        ring_copy(t, 1, 0, 2, 1, y=y_left).start()
+
+    def sums_right(t):
+        core_copy(t, y_right, 2).wait_recv()
+        fill_ring(t, 2, 1, y_right)
+        ring_copy(t, 2, 1, 3, 0, y=y_right).start()
+
+    def sums_near(t):
+        ring_copy(t, 0, 0, 0, None, y=y_right).wait_recv()
+        fill_ring(t, 2, 0, y_right, True)
+        ring_copy(t, 2, 0, 4, 0, y=y_right).start()
+        ring_copy(t, 0, 1, 1, None, y=y_left).wait_recv()
+        fill_ring(t, 1, 1, y_left, True)
+        ring_copy(t, 1, 1, 5, 1, y=y_left).start()
+
+    def sums_sent(t):
+        n, cols = place(t)
+        all_sent(from_core.at[n, :, :, cols], c_send.at[t])
+        all_sent(to_ring.at[n, :, :, :, cols], r_send.at[t])
+
+    def sums_wait(t):
+        core_copy(t, y, 3).wait_recv()
         for side in (0, 1):
             for q in (0, 1):
-                near_wait(n, side, q)
-
-    def own_sum(n, q, at_row):
-        total = chip_sum(n, y, q * QUARTER + at_row)
+                k = ((4, 3), (2, 5))[side][q]
+                ring_copy(t, 0, q, k, side, y=y_right).wait_recv()
+
+    def own_sum(t, q, at_row):
+        n, cols = place(t)
+        total = chip_sum(t, y, q * QUARTER + at_row)
         for side in (0, 1):
-            total = total + near_in[n, side, q, at_row : at_row + 16, :].astype(F32)
+            total = total + near_in[n, side, q, at_row : at_row + 16, cols].astype(F32)
         return total
 
     def first_norm(h):
@@ -517,24 +561,26 @@
                     carry[yq, s, 0:1, lanes] = state[HALF - 1 :]
                 recurred[h, yq, s * HALF : (s + 1) * HALF, lanes] = state.astype(BF16)
 
-    def product(n, g, left, table, order):
+    def step_product(t, g):
+        n, lo, hi = SUMS[t]
+        left, table = (recurred, out_g) if n < 2 else (hidden, down_g)
         rows = jnp.concatenate([left[n % 2, yq] for yq in group(g)], axis=0)
-        for zq in range(RING):
-            w = jnp.concatenate([table[zq, xq] for xq in range(RING)], axis=1)
-            term = jnp.dot(rows, w, preferred_element_type=F32).astype(BF16)
+        for b in range(lo, hi, 4):
+            end = min(b + 4, hi)
+            w = []
+            for d in range(b, end):
+                if n < 2:
+                    w.append(table[d // RING, d % RING])
+                else:
+                    w.append(table[nxt("z", BLOCKS[d][0]), nxt("x", BLOCKS[d][1])])
+            term = jnp.dot(rows, jnp.concatenate(w, axis=1), preferred_element_type=F32)
+            term = term.astype(BF16)
             for j, yq in enumerate(group(g)):
                 for s in range(2):
-                    lo = (2 * j + s) * HALF
-                    partial[n, yq, s, :, zq * 512 : (zq + 1) * 512] = term[lo : lo + HALF]
-        for j, k in order:
-            core_copy(n, group(g)[j], k).start()
-
-    def step_product(n, g):
-        order = ((1, 2), (0, 3)) if g == 0 else ((1, 0), (0, 1))
-        if n < 2:
-            product(n, g, recurred, out_g, order)
-        else:
-            product(n, g, hidden, down_g, order)
+                    at_row = (2 * j + s) * HALF
+                    partial[n, yq, s, :, b * 128 : end * 128] = term[at_row : at_row + HALF]
+        for j, k in ((1, 2), (0, 3)) if g == 0 else ((1, 0), (0, 1)):
+            core_copy(t, group(g)[j], k).start()
 
     def second_norm(h):
         sums_wait(h)
@@ -581,15 +627,18 @@
                     else:
                         hidden[h, yq, out, 640:704] = unit[:, :64]
 
-    def finish(h):
-        sums_wait(2 + h)
+    def finish(t):
+        n, lo, hi = SUMS[t]
+        sums_wait(t)
         for q in (0, 1):
             for at_row in range(0, QUARTER, 16):
-                lo = h * HALF + q * QUARTER + at_row
-                here = slice(lo, lo + 16)
-                total = middle[here, :].astype(F32) + own_sum(2 + h, q, at_row)
-                result[here, :] = total.astype(BF16)
-        result_copy(h).start()
+                here = pl.ds((n - 2) * HALF + q * QUARTER + at_row, 16)
+                total = own_sum(t, q, at_row)
+                for b in range(lo, hi):
+                    at_col = nxt("z", BLOCKS[b][0]) * 512 + nxt("x", BLOCKS[b][1]) * 128
+                    cols = pl.ds(pl.multiple_of(at_col, 128), 128)
+                    part = total[:, (b - lo) * 128 : (b - lo + 1) * 128]
+                    result[here, cols] = (middle[here, cols].astype(F32) + part).astype(BF16)
 
     own_copy(4).wait()
     own_copy(7).wait()
@@ -608,8 +657,8 @@
     def sent():
         for n in range(4):
             rows_sent(n)
-            if n < 3:
-                sums_sent(n)
+        for t in range(5):
+            sums_sent(t)
         for i in range(4):
             weights_sent(i)
 
@@ -618,7 +667,8 @@
         "F1": first_forward,
         "S2": second_send,
         "F2": second_forward,
-        "D": weights_done,
+        "DA": weights_near,
+        "DB": weights_far,
         "RS": rows_send,
         "R1": rows_first,
         "R2": rows_second,
@@ -636,9 +686,7 @@
     }
     for name, *where in ORDER:
         steps[name](*where)
-    sums_sent(3)
-    result_copy(0).wait()
-    result_copy(1).wait()
+    sums_sent(5)
 
 
 def shards(
@@ -677,7 +725,6 @@
             pltpu.VMEM((1, *decay_rate.shape), F32),
             pltpu.VMEM((1, width), F32),
             pltpu.VMEM(ffn_taps.shape, F32),
-            pltpu.VMEM(resid.shape, BF16),
             pltpu.VMEM((RING, RING, *in_weight.shape), BF16),
             pltpu.VMEM((RING, RING, *out_weight.shape), BF16),
             pltpu.VMEM((RING, RING, up_gate_w.shape[0], 2 * units), BF16),
@@ -698,15 +745,15 @@
             pltpu.VMEM((4, 2, QUARTER, width), BF16),
             pltpu.VMEM((4, 2, 2, QUARTER, width), BF16),
             pltpu.VMEM((SEQ, width), BF16),
-            dma((4, 4, 6)),
-            dma((4, 4, 6)),
-            dma((16,)),
+            dma((4, 2)),
+            dma((4, max(PIECES), 6)),
+            dma((14,)),
+            dma((4, 2)),
             dma((4, 14)),
-            dma((4, 14)),
-            dma((4, 4)),
-            dma((4, 4)),
-            dma((4, 6)),
-            dma((4, 6)),
+            dma((6,)),
+            dma((6, 4)),
+            dma((6,)),
+            dma((6, 6)),
         ],
         compiler_params=pltpu.CompilerParams(
             collective_id=0, has_side_effects=True, vmem_limit_bytes=56 * 1024 * 1024

time: 93.5 us -> 91.2 us (0.975)
  Pallas kernels: 92.6 us -> 90.3 us
    pallas_call x1, Pallas kernels: 92.6 us -> 90.3 us  [shards(): pl.pallas_call(kernel, name='layer', out_shape=pltpu.VMEM(resid.shape, BF...]
where the time goes in v4:
time: 91.2 us; the launch traced here: 91.1 us
  Pallas kernels  90.3 us (99%)
    pallas_call x1, Pallas kernels, shards(): pl.pallas_call(kernel, name='layer', out_shape=pltpu.VMEM(resid.shape, BF...  90.3 us

profile of v4, /device:TPU:1, one launch (start us, length us, event | category | flops | bytes accessed | tf_op | source)
XLA Modules:
  0.0 91.1 jit_solution(7871404609168227475)
XLA Ops:
  0.0 90.3 %layer.1 = bf16[128,2048]{1,0:T(8,128)(2,1)S(1)} custom-call(bf16[128,2048]{1,0:T(8,128)(2,1)} %resid_hbm.1, f32[1,2048]{1,0:T(1,128)} %bitcast.7, bf16[128,256]{1,0:T(8,128)(2,1)} %in_w.1, f32[4,256]{1,0:T(4,128)} %conv_taps_hbm.1, bf16[4,64,64]{2,1,0:T(8,128)(2,1)} %recur_w_hbm.1, bf16[4,64,64]{2,1,0:T(8,128)(2,1)} %input_w_hbm.1, f32[1,256]{1,0:T(1,128)} %bitcast.9, ...), custom_call_target="tpu_custom_call" | custom-call | tf_op jit(solution)/shard_map/layer/pallas_call | solution.py:711
  90.3 0.8 copy.15

commit v5 on v4

--- a/solution.py
+++ b/solution.py
@@ -20,152 +20,153 @@
 
 PIECES = (4, 4, 4, 4)
 X_FIRST = (2, 2, 2, 2)
+DIRECT = (True, True, False, False)
 SUMS = ((0, 0, 16), (1, 0, 16), (2, 0, 9), (3, 0, 9), (2, 9, 16), (3, 9, 16))
 BLOCKS = tuple(
     sorted(((dz, dx) for dz in (0, 1, -1, 2) for dx in (0, 1, -1, 2)), key=lambda d: 2 in d)
 )
 ORDER = (
+    ("S1", 3, 3),
+    ("S1", 2, 1),
+    ("S1", 1, 2),
+    ("S1", 0, 0),
+    ("RS", 0),
+    ("S1", 0, 2),
+    ("S1", 0, 3),
+    ("S1", 1, 0),
     ("S1", 0, 1),
-    ("S1", 1, 0),
+    ("S1", 1, 1),
     ("S1", 1, 3),
-    ("RS", 0),
-    ("S1", 0, 3),
-    ("S1", 0, 0),
-    ("S1", 1, 2),
-    ("S1", 0, 2),
-    ("S1", 1, 1),
     ("S1", 2, 2),
+    ("F1", 0, 0),
     ("S1", 2, 0),
+    ("F1", 0, 2),
+    ("RS", 1),
+    ("S1", 2, 3),
+    ("F1", 0, 3),
     ("F1", 1, 3),
+    ("F1", 0, 1),
+    ("S2", 0, 0),
     ("F1", 1, 0),
-    ("F1", 0, 3),
-    ("F1", 0, 0),
-    ("S1", 2, 3),
-    ("RS", 1),
-    ("S1", 2, 1),
+    ("S2", 0, 2),
+    ("S2", 0, 3),
+    ("S2", 1, 3),
+    ("S2", 1, 0),
+    ("F1", 1, 2),
+    ("S2", 1, 2),
+    ("F1", 1, 1),
+    ("S2", 0, 1),
+    ("F1", 2, 0),
+    ("F2", 0, 0),
+    ("S2", 1, 1),
+    ("F2", 0, 2),
+    ("R1", 0),
+    ("R2", 0),
     ("S1", 3, 1),
-    ("F1", 1, 2),
-    ("F1", 0, 2),
-    ("F1", 0, 1),
+    ("F2", 0, 3),
+    ("F1", 2, 3),
+    ("F1", 2, 1),
     ("F1", 2, 2),
-    ("F1", 2, 0),
-    ("S2", 0, 3),
-    ("F1", 1, 1),
-    ("S2", 1, 0),
-    ("S2", 0, 0),
-    ("S2", 0, 1),
-    ("S2", 0, 2),
-    ("S2", 1, 3),
-    ("S2", 1, 2),
-    ("S2", 1, 1),
-    ("R1", 0),
-    ("F1", 2, 3),
-    ("F1", 3, 1),
-    ("F2", 0, 3),
-    ("R2", 1),
-    ("F2", 0, 0),
-    ("F2", 0, 2),
     ("F2", 0, 1),
     ("F2", 1, 1),
     ("R1", 1),
+    ("F2", 1, 2),
+    ("F2", 1, 0),
     ("F2", 1, 3),
-    ("F2", 1, 0),
+    ("R2", 1),
+    ("S1", 3, 0),
     ("R3", 0),
-    ("F2", 1, 2),
-    ("F1", 2, 1),
     ("S1", 3, 2),
-    ("R2", 0),
-    ("S1", 3, 0),
-    ("S1", 3, 3),
     ("S2", 2, 0),
-    ("S2", 2, 2),
+    ("DA", 0),
     ("DA", 1),
-    ("DA", 0),
+    ("F1", 3, 1),
+    ("S2", 2, 3),
     ("DB", 0),
     ("rec", 0, 1),
-    ("R3", 1),
     ("DB", 1),
     ("prod", 0, 1),
     ("rec", 0, 0),
     ("sfar", 0),
+    ("R3", 1),
+    ("F1", 3, 2),
+    ("S2", 2, 1),
     ("prod", 0, 0),
-    ("S2", 2, 3),
     ("sleft", 0),
-    ("F1", 3, 3),
-    ("F1", 3, 2),
     ("sright", 0),
+    ("S2", 2, 2),
     ("rec", 1, 1),
-    ("S2", 2, 1),
     ("prod", 1, 1),
     ("near", 0),
+    ("rec", 1, 0),
     ("sfar", 1),
+    ("prod", 1, 0),
+    ("sleft", 1),
+    ("F2", 2, 0),
+    ("F2", 2, 3),
+    ("S2", 3, 1),
+    ("sright", 1),
     ("S2", 3, 2),
-    ("F2", 2, 0),
     ("F1", 3, 0),
-    ("S2", 3, 1),
-    ("rec", 1, 0),
-    ("sleft", 1),
+    ("near", 1),
+    ("F1", 3, 3),
+    ("norm2", 0),
+    ("RS", 2),
+    ("F2", 2, 1),
     ("F2", 2, 2),
-    ("prod", 1, 0),
-    ("sright", 1),
-    ("norm2", 0),
-    ("near", 1),
-    ("RS", 2),
-    ("F2", 2, 3),
-    ("F2", 2, 1),
+    ("R1", 2),
+    ("S2", 3, 3),
+    ("S2", 3, 0),
     ("norm2", 1),
-    ("S2", 3, 3),
+    ("RS", 3),
+    ("F2", 3, 2),
+    ("R2", 2),
+    ("R3", 2),
     ("DA", 2),
-    ("R1", 2),
-    ("S2", 3, 0),
+    ("DB", 2),
     ("F2", 3, 1),
-    ("RS", 3),
-    ("DB", 2),
-    ("R2", 2),
-    ("F2", 3, 2),
-    ("R3", 2),
     ("feed", 0, 0),
+    ("F2", 3, 0),
+    ("F2", 3, 3),
     ("R1", 3),
-    ("F2", 3, 3),
-    ("F2", 3, 0),
     ("DA", 3),
     ("feed", 0, 1),
+    ("prod", 2, 0),
+    ("prod", 2, 1),
     ("R2", 3),
-    ("prod", 2, 1),
-    ("prod", 2, 0),
     ("sfar", 2),
     ("R3", 3),
+    ("DB", 3),
+    ("prod", 4, 1),
+    ("prod", 4, 0),
     ("sright", 2),
     ("sleft", 2),
-    ("DB", 3),
-    ("prod", 4, 1),
+    ("sfar", 4),
     ("feed", 1, 1),
-    ("sfar", 4),
+    ("sright", 4),
+    ("sleft", 4),
+    ("prod", 3, 1),
     ("near", 2),
     ("prod", 5, 1),
-    ("prod", 4, 0),
-    ("prod", 3, 1),
+    ("near", 4),
+    ("sfar", 3),
+    ("feed", 1, 0),
+    ("prod", 3, 0),
     ("sfar", 5),
-    ("sright", 4),
-    ("sleft", 4),
-    ("near", 4),
-    ("feed", 1, 0),
-    ("sfar", 3),
     ("sleft", 5),
+    ("sright", 3),
+    ("sleft", 3),
+    ("fin", 2),
     ("prod", 5, 0),
-    ("fin", 2),
+    ("near", 3),
+    ("sent",),
+    ("fin", 4),
     ("sright", 5),
     ("near", 5),
-    ("sleft", 3),
-    ("prod", 3, 0),
-    ("sright", 3),
-    ("fin", 4),
-    ("near", 3),
-    ("sent",),
+    ("fin", 3),
     ("fin", 5),
-    ("fin", 3),
 )
-WAITED = {0: 3, 1: 0, 3: 2}
+WAITED = {0: 0, 1: 3, 3: 1}
 
 
 def remote(src, dst, send_sem, recv_sem, **device):
@@ -281,7 +282,7 @@
 
     barrier = pltpu.get_barrier_semaphore()
     for axis in ("z", "x", "y"):
-        for by in (1, -1):
+        for by in (1, -1) if axis == "y" else (1, -1, 2):
             pl.semaphore_signal(
                 barrier, inc=1, device_id={axis: nxt(axis, by)}, device_id_type=MESH
             )
@@ -315,7 +316,7 @@
         src = weights[i][0]
         axis = axes_of(i, p)[0]
         here = slot(i, p, axis, 0)
-        for k, by in ((0, 1), (1, -1)):
+        for k, by in ((0, 1), (1, -1), (2, 2))[: 3 if DIRECT[i] else 2]:
             w_copy(i, p, here if src is None else src.at[piece(i, p)], here, k, axis, by).start()
 
     def first_wait(i, p, k):
@@ -329,7 +330,8 @@
         first_wait(i, p, k)
         by = 1 if k == 0 else -1
         there = slot(i, p, axis, -by)
-        w_copy(i, p, there, there, 2, axis, by).start()
+        if not DIRECT[i]:
+            w_copy(i, p, there, there, 2, axis, by).start()
 
     def second_send(i, p):
         if p == WAITED.get(i):
@@ -652,7 +654,7 @@
     first_norm(1)
     for i in (10, 11, 12, 13):
         own_copy(i).wait()
-    pl.semaphore_wait(barrier, 7)
+    pl.semaphore_wait(barrier, 9)
 
     def sent():
         for n in range(4):

time: 91.2 us -> 90.9 us (level)
  no operation moved by 1% of the time
where the time goes in v5:
time: 90.9 us; the launch traced here: 90.7 us
  Pallas kernels  89.9 us (99%)
    pallas_call x1, Pallas kernels, shards(): pl.pallas_call(kernel, name='layer', out_shape=pltpu.VMEM(resid.shape, BF...  89.9 us

profile of v5, /device:TPU:1, one launch (start us, length us, event | category | flops | bytes accessed | tf_op | source)
XLA Modules:
  0.0 90.7 jit_solution(11971088168035591050)
XLA Ops:
  0.0 89.9 %layer.1 = bf16[128,2048]{1,0:T(8,128)(2,1)S(1)} custom-call(bf16[128,2048]{1,0:T(8,128)(2,1)} %resid_hbm.1, f32[1,2048]{1,0:T(1,128)} %bitcast.7, bf16[128,256]{1,0:T(8,128)(2,1)} %in_w.1, f32[4,256]{1,0:T(4,128)} %conv_taps_hbm.1, bf16[4,64,64]{2,1,0:T(8,128)(2,1)} %recur_w_hbm.1, bf16[4,64,64]{2,1,0:T(8,128)(2,1)} %input_w_hbm.1, f32[1,256]{1,0:T(1,128)} %bitcast.9, ...), custom_call_target="tpu_custom_call" | custom-call | tf_op jit(solution)/shard_map/layer/pallas_call | solution.py:713
  89.9 0.8 copy.15

commit v6 on v5

--- a/solution.py
+++ b/solution.py
@@ -27,7 +27,6 @@
 )
 ORDER = (
     ("S1", 3, 3),
-    ("S1", 2, 1),
     ("S1", 1, 2),
     ("S1", 0, 0),
     ("RS", 0),
@@ -37,6 +36,8 @@
     ("S1", 0, 1),
     ("S1", 1, 1),
     ("S1", 1, 3),
+    ("local",),
+    ("S1", 2, 1),
     ("S1", 2, 2),
     ("F1", 0, 0),
     ("S1", 2, 0),
@@ -60,6 +61,7 @@
     ("F2", 0, 0),
     ("S2", 1, 1),
     ("F2", 0, 2),
+    ("maps",),
     ("R1", 0),
     ("R2", 0),
     ("S1", 3, 1),
@@ -645,16 +647,18 @@
     own_copy(4).wait()
     own_copy(7).wait()
     first_norm(0)
-    own_copy(5).wait()
-    own_copy(6).wait()
-    turn_up()
-    own_copy(8).wait()
-    own_copy(9).wait()
-    gate_map()
-    first_norm(1)
-    for i in (10, 11, 12, 13):
-        own_copy(i).wait()
     pl.semaphore_wait(barrier, 9)
+
+    def local():
+        own_copy(5).wait()
+        own_copy(6).wait()
+        turn_up()
+        first_norm(1)
+
+    def maps():
+        for i in (8, 9, 10, 11, 12, 13):
+            own_copy(i).wait()
+        gate_map()
 
     def sent():
         for n in range(4):
@@ -665,6 +669,8 @@
             weights_sent(i)
 
     steps = {
+        "local": local,
+        "maps": maps,
         "S1": first_send,
         "F1": first_forward,
         "S2": second_send,

time: 90.9 us -> 90.8 us (level)
  no operation moved by 1% of the time
where the time goes in v6:
time: 90.8 us; the launch traced here: 90.7 us
  Pallas kernels  89.9 us (99%)
    pallas_call x1, Pallas kernels, shards(): pl.pallas_call(kernel, name='layer', out_shape=pltpu.VMEM(resid.shape, BF...  89.9 us

profile of v6, /device:TPU:1, one launch (start us, length us, event | category | flops | bytes accessed | tf_op | source)
XLA Modules:
  0.0 90.7 jit_solution(4410521375531759853)
XLA Ops:
  0.0 89.9 %layer.1 = bf16[128,2048]{1,0:T(8,128)(2,1)S(1)} custom-call(bf16[128,2048]{1,0:T(8,128)(2,1)} %resid_hbm.1, f32[1,2048]{1,0:T(1,128)} %bitcast.7, bf16[128,256]{1,0:T(8,128)(2,1)} %in_w.1, f32[4,256]{1,0:T(4,128)} %conv_taps_hbm.1, bf16[4,64,64]{2,1,0:T(8,128)(2,1)} %recur_w_hbm.1, bf16[4,64,64]{2,1,0:T(8,128)(2,1)} %input_w_hbm.1, f32[1,256]{1,0:T(1,128)} %bitcast.9, ...), custom_call_target="tpu_custom_call" | custom-call | tf_op jit(solution)/shard_map/layer/pallas_call | solution.py:719
  89.9 0.8 copy.15
